TPU v7x, 256 devices: a whole 4x4x8 slice. The times are simulated.
256 devices in a mesh: sp: 16 (over y, x), tp: 16 (over z, core).
Axes of the slice: x: 4, y: 4, z: 8, core: 2. Of those that a mesh axis runs over, the one named last changes fastest.
Arguments:
- ask_preactivation_left: bfloat16 [8192, 2048], P('sp', 'tp'), may hold values from -6 to 6
- keep_preactivation_left: bfloat16 [8192, 2048], P('sp', 'tp'), may hold values from -6 to 6
- keep_bound_complement_left: float32 [2048], P('tp'), may hold values from 0 to 0.1
- ask_preactivation_right: bfloat16 [8192, 4096], P('sp', 'tp'), may hold values from -6 to 6
- keep_preactivation_right: bfloat16 [8192, 4096], P('sp', 'tp'), may hold values from -6 to 6
- keep_bound_complement_right: float32 [4096], P('tp'), may hold values from 0 to 0.1
- payload_entries: bfloat16 [8192, 2048], P('sp', 'tp'), may hold values from -6 to 6
- emission_switch_logits: bfloat16 [8192, 2048], P('sp', 'tp'), may hold values from -6 to 6
- added_log_keep_bias: float32 [8192, 32], P('sp', 'tp'), may hold values from -2.1 to 0
- lanewise_rescale: float32 [64], replicated, may hold values from 0.1 to 1.9
- emission_matrix_alpha: bfloat16 [1024, 2048], P('tp'), may hold values from -0.125 to 0.125
- emission_matrix_beta: bfloat16 [1024, 2048], P('tp'), may hold values from -0.125 to 0.125
- skip_stream: bfloat16 [8192, 2048], P(('sp', 'tp')), may hold values from -6 to 6
- postrecurrence_rescale: float32 [2048], replicated, may hold values from 0.1 to 1.9
- premixture_rescale: float32 [2048], replicated, may hold values from 0.1 to 1.9
- postmixture_rescale: float32 [2048], replicated, may hold values from 0.1 to 1.9
- dispatcher_columns: bfloat16 [2048, 32], P(None, 'sp'), may hold values from -0.125 to 0.125
- switch_matrix: bfloat16 [16, 2048, 4096], P('sp', None, 'tp'), may hold values from -0.125 to 0.125
- expansion_matrix: bfloat16 [16, 2048, 4096], P('sp', None, 'tp'), may hold values from -0.125 to 0.125
- contraction_matrix: bfloat16 [16, 4096, 2048], P('sp', 'tp'), may hold values from -0.125 to 0.125
- item_specialist_cluster: int32 [8192], P(('sp', 'tp')), may hold values from 0 to 15, as said below
Outputs:
- result: bfloat16 [8192, 2048], P(('sp', 'tp'))
Inputs may be any that keep to these rules, and one draw needn't show every extreme that they name: `item_specialist_cluster`: in every aligned block of 32 tokens (the rows of one device) no group is named more than 3 times, and some group exactly 3 times.
All inputs are finite; a program needn't handle non-finite values.
Results may differ from a plain program's by a relative error of at most 0.023.
Values may be sent and summed in bfloat16 or wider, within the bound.
A program may use at most 64 MiB of HBM per device.

v0:
```python
import jax
import jax.numpy as jnp
from jax import lax
from jax.sharding import PartitionSpec as P

FF = 2048
BLOCK_LENGTH = 512


EPSILON = 1e-06
PRECISE = lax.Precision.HIGHEST


def copy_for_each(shard, axis):
    length = lax.axis_size(axis)
    return lax.all_to_all(
        jnp.broadcast_to(shard[None], (length, *shard.shape)), axis, 0, 0, tiled=True
    )


def collected_together(shard, axis):
    leaves = jax.tree.leaves(shard)
    order = sorted(range(len(leaves)), key=lambda k: -leaves[k].size)
    width = (1, *leaves[order[0]].shape)[-1]
    lines = [
        jnp.pad(leaves[k].reshape(-1), (0, -leaves[k].size % width)).reshape(-1, width)
        for k in order
    ]
    both, at, found = (copy_for_each(jnp.concatenate(lines), axis), 0, {})
    for k, line in zip(order, lines):
        piece = both[:, at : at + len(line)].reshape(len(both), -1)
        found[k] = piece[:, : leaves[k].size].reshape(-1, *leaves[k].shape)
        at += len(line)
    numbers = iter(range(len(leaves)))
    return jax.tree.map(lambda _: found[next(numbers)], shard)


def combined_pairwise(pieces, combine):
    while len(jax.tree.leaves(pieces)[0]) > 1:
        pieces = jax.vmap(combine)(
            *(jax.tree.map(lambda part: part[side::2], pieces) for side in (0, 1))
        )
    return jax.tree.map(lambda part: part[0], pieces)


def entering(shard, axis, combine, identity):
    length, index = (lax.axis_size(axis), lax.axis_index(axis))
    passed = jnp.arange(length) < index

    def kept(part, zero, own):
        part = jnp.where(
            passed.reshape(-1, *(1 for _ in own.shape)),
            part.astype(own.dtype),
            jnp.asarray(zero, own.dtype),
        )
        return part

    pieces = collected_together(
        jax.tree.map(
            lambda part, kind: part.astype(kind),
            shard,
            jax.tree.map(lambda a: jnp.bfloat16 if a.dtype == jnp.float32 else a.dtype, shard),
        ),
        axis,
    )
    return combined_pairwise(jax.tree.map(kept, pieces, identity, shard), combine)


def split_up(shard, dim, length):
    before, after = (shard.shape[:dim], shard.shape[dim + 1 :])
    return jnp.moveaxis(shard.reshape(*before, length, -1, *after), dim, 0)


def summed_on_arrival(shard, axis, dim):
    parts = split_up(shard, dim, lax.axis_size(axis))
    arrived = lax.all_to_all(parts, axis, split_axis=0, concat_axis=0, tiled=True)
    return arrived.astype(jnp.float32).sum(axis=0)


def rms_scale(features, gain):
    return (
        features * lax.rsqrt(jnp.mean(features * features, axis=-1, keepdims=True) + EPSILON) * gain
    )


def block_step(carry_state, inputs):
    queries, incoming_key_rows, value_row_block, inside = inputs
    length = queries.shape[0]
    causal = lax.broadcasted_iota(jnp.int32, (length, length), 0) >= lax.broadcasted_iota(
        jnp.int32, (length, length), 1
    )
    q_decayed = queries * jnp.exp(inside)
    k_grown = incoming_key_rows * jnp.exp(-inside)
    scores = jnp.einsum("thd,shd->hts", q_decayed, k_grown, precision=PRECISE)
    scores = jnp.where(causal[None], scores, jnp.zeros_like(scores))
    outputs = jnp.einsum("hts,shv->thv", scores, value_row_block, precision=PRECISE)
    outputs = outputs + jnp.einsum("thd,hdv->thv", q_decayed, carry_state, precision=PRECISE)
    last_decay = inside[-1]
    fresh_state = jnp.einsum(
        "shd,shv->hdv",
        incoming_key_rows * jnp.exp(last_decay[None] - inside),
        value_row_block,
        precision=PRECISE,
    )
    return (jnp.exp(last_decay)[:, :, None] * carry_state + fresh_state, outputs)


def group_preparation(query_vector, forget_gate, lower_margin, spike_value, value_row_block):
    entity_amount_global = query_vector.shape[0]
    attention_unit_amount = spike_value.shape[1]
    recurrent_state_width = query_vector.shape[1] // attention_unit_amount
    block_total_count = entity_amount_global // BLOCK_LENGTH
    block_shape = (block_total_count, BLOCK_LENGTH, attention_unit_amount, recurrent_state_width)
    queries = jax.nn.silu(query_vector.astype(jnp.float32)).reshape(block_shape)
    incoming_key_rows = lower_margin.reshape(
        attention_unit_amount, recurrent_state_width
    ) * jax.nn.sigmoid(-forget_gate.astype(jnp.float32)).reshape(block_shape)
    logarithm_decay = jnp.log1p(-incoming_key_rows) + spike_value.reshape(
        block_total_count, BLOCK_LENGTH, attention_unit_amount, 1
    )
    inside = jnp.cumsum(logarithm_decay, axis=1)
    block_totals = inside[:, -1]
    before = jnp.cumsum(block_totals, axis=0) - block_totals
    running = before[:, None] + inside
    blocked_values = value_row_block.reshape(
        block_total_count, BLOCK_LENGTH, attention_unit_amount, -1
    )
    return (
        queries,
        incoming_key_rows,
        blocked_values,
        inside,
        running,
        jnp.sum(block_totals, axis=0),
    )


def run_blocks(setup, start_state):
    final_state, outputs = lax.scan(
        block_step, start_state, (setup[0], setup[1], setup[2], setup[3])
    )
    return (final_state, outputs.reshape(-1, outputs.shape[2], outputs.shape[3]))


def summary(setup):
    weighted_keys = setup[1] * jnp.exp(setup[5] - setup[4])
    return jnp.einsum("nlhd,nlhv->hdv", weighted_keys, setup[2], precision=PRECISE)


def combine_states(earlier, later):
    return (
        earlier[0] + later[0],
        jnp.exp(later[0])[:, :, None] * earlier[1] + later[1],
        earlier[2] + later[2],
        jnp.exp(later[2])[:, :, None] * earlier[3] + later[3],
    )


def carry_states(preparation_first, state_a, preparation_second, state_b):
    summaries = (preparation_first[5], state_a, preparation_second[5], state_b)
    identity = tuple((jnp.zeros_like(member) for member in summaries))
    incoming = entering(summaries, "sp", combine_states, identity)
    return (incoming[1], incoming[3])


def finish(outputs, gate_rows, lanewise_rescale):
    scaled = rms_scale(outputs, lanewise_rescale) * jax.nn.sigmoid(gate_rows.astype(jnp.float32))
    return scaled.astype(jnp.bfloat16).reshape(outputs.shape[0], -1)


def expert_rows(
    piece, dispatcher_columns, switch_matrix, expansion_matrix, contraction_matrix, member
):
    flat_rows = piece.reshape(-1, piece.shape[-1])
    scores = jax.nn.sigmoid(
        jnp.dot(flat_rows, dispatcher_columns, preferred_element_type=jnp.float32)
    )
    weights = scores / jnp.sum(scores, axis=1, keepdims=True)
    picked = (
        lax.broadcasted_iota(jnp.int32, (1, dispatcher_columns.shape[1]), 1) == member
    ).astype(jnp.float32)
    member_weight = jnp.sum(weights * picked, axis=1, keepdims=True)
    gate_proj = jnp.dot(flat_rows, switch_matrix[0], preferred_element_type=jnp.float32)
    up_proj = jnp.dot(flat_rows, expansion_matrix[0], preferred_element_type=jnp.float32)
    hidden = (jax.nn.silu(gate_proj) * up_proj).astype(jnp.bfloat16)
    product = jnp.dot(hidden, contraction_matrix[0], preferred_element_type=jnp.float32)
    return (member_weight * product).astype(jnp.bfloat16).reshape(piece.shape)


def shards(
    ask_preactivation_left,
    keep_preactivation_left,
    keep_bound_complement_left,
    ask_preactivation_right,
    keep_preactivation_right,
    keep_bound_complement_right,
    payload_entries,
    emission_switch_logits,
    added_log_keep_bias,
    lanewise_rescale,
    emission_matrix_alpha,
    emission_matrix_beta,
    skip_stream,
    postrecurrence_rescale,
    premixture_rescale,
    postmixture_rescale,
    dispatcher_columns,
    switch_matrix,
    expansion_matrix,
    contraction_matrix,
    item_specialist_cluster,
):
    entity_amount_global = ask_preactivation_left.shape[0]
    attention_unit_amount = added_log_keep_bias.shape[1] // 2
    value_width = payload_entries.shape[1] // (2 * attention_unit_amount)
    routing_assignment = added_log_keep_bias.reshape(entity_amount_global, attention_unit_amount, 2)
    content_coupling = payload_entries.astype(jnp.float32).reshape(
        entity_amount_global, attention_unit_amount, 2, value_width
    )
    gate_pair = emission_switch_logits.reshape(
        entity_amount_global, attention_unit_amount, 2, value_width
    )
    preparation_first = group_preparation(
        ask_preactivation_left,
        keep_preactivation_left,
        keep_bound_complement_left,
        routing_assignment[:, :, 0],
        content_coupling[:, :, 0],
    )
    preparation_second = group_preparation(
        ask_preactivation_right,
        keep_preactivation_right,
        keep_bound_complement_right,
        routing_assignment[:, :, 1],
        content_coupling[:, :, 1],
    )
    carried_a, carried_b = carry_states(
        preparation_first,
        summary(preparation_first),
        preparation_second,
        summary(preparation_second),
    )
    outputs_a = run_blocks(preparation_first, carried_a)[1]
    outputs_b = run_blocks(preparation_second, carried_b)[1]
    head_a = finish(outputs_a, gate_pair[:, :, 0], lanewise_rescale)
    head_b = finish(outputs_b, gate_pair[:, :, 1], lanewise_rescale)
    row_count = skip_stream.shape[0]
    term = jnp.dot(head_a, emission_matrix_alpha, preferred_element_type=jnp.float32)
    term = term + jnp.dot(head_b, emission_matrix_beta, preferred_element_type=jnp.float32)
    mixed = summed_on_arrival(
        lax.optimization_barrier(term.astype(jnp.bfloat16))
        .astype(jnp.float32)
        .astype(jnp.bfloat16),
        "tp",
        0,
    )
    h_mid = (skip_stream.astype(jnp.float32) + rms_scale(mixed, postrecurrence_rescale)).astype(
        jnp.bfloat16
    )
    normed = rms_scale(h_mid.astype(jnp.float32), premixture_rescale).astype(jnp.bfloat16)
    groups = lax.axis_size("sp")
    capacity = (9 * row_count + 8 * groups - 1) // (8 * groups)
    member = item_specialist_cluster[:, None] == lax.broadcasted_iota(
        jnp.int32, (row_count, groups), 1
    )
    member_count = member.astype(jnp.int32)
    slot_rank = jnp.sum(jnp.cumsum(member_count, axis=0) * member_count, axis=1) - 1
    slot_id = item_specialist_cluster * capacity + slot_rank
    placing = (
        slot_id[None, :] == lax.broadcasted_iota(jnp.int32, (groups * capacity, row_count), 0)
    ).astype(jnp.bfloat16)
    outgoing = jnp.dot(placing, normed, preferred_element_type=jnp.float32).astype(jnp.bfloat16)
    outgoing = outgoing.reshape(groups, capacity, normed.shape[1])
    incoming = lax.all_to_all(outgoing, "sp", split_axis=0, concat_axis=0, tiled=True)
    own_member = lax.axis_index("tp") * switch_matrix.shape[2] // FF
    partials = expert_rows(
        lax.all_gather(incoming, "tp", axis=0, tiled=True),
        dispatcher_columns,
        switch_matrix,
        expansion_matrix,
        contraction_matrix,
        own_member,
    )
    summed = summed_on_arrival(partials.astype(jnp.float32).astype(jnp.bfloat16), "tp", 0)
    returned = lax.all_to_all(
        summed.astype(jnp.bfloat16), "sp", split_axis=0, concat_axis=0, tiled=True
    )
    routed = jnp.einsum(
        "sr,sd->rd",
        placing,
        returned.reshape(groups * capacity, -1),
        preferred_element_type=jnp.float32,
    )
    return (h_mid.astype(jnp.float32) + rms_scale(routed, postmixture_rescale)).astype(jnp.bfloat16)


def solution(mesh):
    placed = (
        P("sp", "tp"),
        P("sp", "tp"),
        P("tp"),
        P("sp", "tp"),
        P("sp", "tp"),
        P("tp"),
        P("sp", "tp"),
        P("sp", "tp"),
        P("sp", "tp"),
        P(),
        P("tp", None),
        P("tp", None),
        P(("sp", "tp"), None),
        P(),
        P(),
        P(),
        P(None, "sp"),
        P("sp", None, "tp"),
        P("sp", None, "tp"),
        P("sp", "tp", None),
        P(("sp", "tp")),
    )
    return jax.shard_map(
        shards, mesh=mesh, in_specs=placed, out_specs=P(("sp", "tp"), None), check_vma=False
    )
```

profile of v0, /device:TPU:2, one launch (start us, length us, event | category | flops | bytes accessed | tf_op | source)
XLA Modules:
  0.0 302.5 jit_solution(16510124631730484713)
XLA Ops:
  6.5 0.8 fusion.98
  7.3 1.1 log-plus-one_add_fusion.1
  8.4 0.2 fusion.40
  8.8 1.3 log-plus-one_add_fusion
  10.2 0.3 fusion.22
  10.5 0.1 copy.92
  10.8 0.1 copy.90
  11.0 0.1 convert_element_type.163
  11.1 0.1 copy.94
  11.3 0.1 copy.93
  11.4 0.3 convolution_convert_fusion.2
  11.7 0.5 convolution_convert_fusion.1
  12.3 1.1 broadcast_in_dim.64
  13.5 7.5 %all-to-all-start = ((bf16[16,390,64]{1,2,0:T(8,128)(2,1)}), bf16[16,390,64]{1,2,0:T(8,128)(2,1)S(1)}, u32[]{:S(2)}, u32[]{:S(2)}) async-start(bf16[16,390,64]{1,2,0:T(8,128)(2,1)} %broadcast_in_dim.64), calls=%async_computation | async-start | bytes 2097152 | tf_op jit(solution)/shard_map/all_to_all | solution.py:16
  21.0 1.0 copy.97
  22.0 2.3 convolution_select_fusion
  24.4 1.3 convolution_bitcast_fusion
  25.7 1.1 convolution_select_fusion.1
  26.8 9.9 %all-to-all-done = bf16[16,390,64]{1,2,0:T(8,128)(2,1)S(1)} async-done(((bf16[16,390,64]{1,2,0:T(8,128)(2,1)}), bf16[16,390,64]{1,2,0:T(8,128)(2,1)S(1)}, u32[]{:S(2)}, u32[]{:S(2)}) %all-to-all-start) | async-done | bytes 798752 | tf_op jit(solution)/shard_map/all_to_all | solution.py:16
  36.7 0.1 slice.203
  36.9 0.2 copy.104
  37.2 0.6 fusion.97
  37.9 0.6 fusion.99
  38.5 0.6 slice.164
  39.1 0.6 slice.163
  39.7 0.2 copy.105
  39.9 0.1 reshape.559
  40.0 0.7 broadcast_select_fusion
  40.8 0.7 fusion.100
  41.5 0.7 select_bitcast_fusion.1
  42.3 0.7 slice_add_fusion.2
  43.0 0.7 slice_add_fusion.4
  43.7 1.5 fusion.58
  45.3 0.7 multiply_reduce_fusion.3
  46.0 0.1 select_bitcast_fusion
  46.4 0.8 multiply_reduce_fusion.2
  47.2 0.8 fusion.64
  48.0 2.2 add_convert_fusion
  50.2 8.7 %all-to-all-start.1 = ((bf16[16,32,2048]{2,1,0:T(8,128)(2,1)}), bf16[16,32,2048]{2,1,0:T(8,128)(2,1)S(1)}, u32[]{:S(2)}, u32[]{:S(2)}) async-start(bf16[16,32,2048]{2,1,0:T(8,128)(2,1)} %bitcast.206), calls=%async_computation.1 | async-start | bytes 4194304 | tf_op jit(solution)/shard_map/all_to_all | solution.py:76
  59.1 0.2 select_reduce_fusion
  59.3 48.9 %all-to-all-done.1 = bf16[16,32,2048]{2,1,0:T(8,128)(2,1)S(1)} async-done(((bf16[16,32,2048]{2,1,0:T(8,128)(2,1)}), bf16[16,32,2048]{2,1,0:T(8,128)(2,1)S(1)}, u32[]{:S(2)}, u32[]{:S(2)}) %all-to-all-start.1) | async-done | bytes 2097184 | tf_op jit(solution)/shard_map/all_to_all | solution.py:76
  108.2 0.4 convert_reduce_fusion
  108.5 0.1 multiply_reduce_fusion.1
  108.7 0.2 fusion.34
  108.9 0.3 convolution_convert_fusion
  109.2 0.1 reshape.552
  109.3 12.5 %all_to_all.25 = bf16[16,3,2048]{2,1,0:T(4,128)(2,1)S(1)} all-to-all(bf16[16,3,2048]{2,1,0:T(4,128)(2,1)S(1)} %reshape.552), channel_id=1, replica_groups=mesh['sp'=16,'tp'=16] {'sp'}, dimensions={0} | all-to-all | bytes 393216 | tf_op jit(solution)/shard_map/all_to_all | solution.py:274
  121.8 0.8 copy.100
  122.7 36.6 %all-gather.2.cloned.1.call-done = bf16[256,3,2048]{2,0,1:T(8,128)(2,1)} async-done(((bf16[16,3,2048]{2,0,1:T(8,128)(2,1)}), bf16[256,3,2048]{2,0,1:T(8,128)(2,1)}) %all-gather.2.cloned.1.call-update) | async-done | bytes 3145744 | tf_op jit(solution)/shard_map/all_gather | solution.py:277
  159.3 6.5 %copy.101 = bf16[256,3,2048]{2,1,0:T(4,128)(2,1)} copy(bf16[256,3,2048]{2,0,1:T(8,128)(2,1)} %all-gather.2.cloned.1.call-done) | data formatting | bytes 6291456 | tf_op jit(solution)/shard_map/all_gather | solution.py:277
  165.8 8.8 %reshape.553 = bf16[768,2048]{1,0:T(8,128)(2,1)} reshape(bf16[256,3,2048]{2,1,0:T(4,128)(2,1)} %copy.101) | data formatting | bytes 6291456 | tf_op jit(solution)/shard_map/reshape | solution.py:174
  174.7 3.0 divide_reduce_fusion
  177.7 0.1 copy-done.25
  177.8 1.0 fusion.9
  178.9 7.2 %multiply_convert_fusion = bf16[768,2048]{1,0:T(8,128)(2,1)} fusion(f32[768]{0:T(1024)S(1)} %multiply_reduce_fusion.4, bf16[768,2048]{1,0:T(8,128)(2,1)} %reshape.553, bf16[1,256,2048]{2,1,0:T(8,128)(2,1)S(1)} %copy-done, bf16[1,2048,256]{2,1,0:T(8,128)(2,1)} %param.39, f32[768,256]{1,0:T(8,128)S(1)} %fusion.9), kind=kOutput, calls=%fused_computation | convolution fusion | flops 1614938112 | bytes 9178112 | tf_op jit(solution)/shard_map/dot_general | solution.py:186
  186.0 9.1 %reshape.554 = bf16[16,16,3,2048]{3,2,1,0:T(4,128)(2,1)} reshape(bf16[768,2048]{1,0:T(8,128)(2,1)} %multiply_convert_fusion) | data formatting | bytes 6291456 | tf_op jit(solution)/shard_map/reshape | solution.py:71
  195.1 4.7 %copy.102 = bf16[16,16,3,2048]{3,1,2,0:T(8,128)(2,1)S(1)} copy(bf16[16,16,3,2048]{3,2,1,0:T(4,128)(2,1)} %reshape.554) | data formatting | bytes 6291456 | tf_op jit(solution)/shard_map/reshape | solution.py:71
  199.8 76.4 %all_to_all.26 = bf16[16,16,3,2048]{3,1,2,0:T(8,128)(2,1)} all-to-all(bf16[16,16,3,2048]{3,1,2,0:T(8,128)(2,1)S(1)} %copy.102), channel_id=1, replica_groups=mesh['sp'=16,'tp'=16] {'tp'}, dimensions={0} | all-to-all | bytes 6291456 | tf_op jit(solution)/shard_map/all_to_all | solution.py:76
  276.3 2.5 reduce_sum.109
  278.8 0.2 copy.103
  279.0 15.4 %all_to_all.27 = bf16[16,3,2048]{2,1,0:T(4,128)(2,1)S(1)} all-to-all(bf16[16,3,2048]{2,1,0:T(4,128)(2,1)S(1)} %copy.103), channel_id=1, replica_groups=mesh['sp'=16,'tp'=16] {'sp'}, dimensions={0} | all-to-all | bytes 393216 | tf_op jit(solution)/shard_map/all_to_all | solution.py:285
  294.4 0.2 reshape.555
  294.5 0.3 multiply_reduce_fusion
  294.9 0.8 fusion.37
  (109 shorter events, 1.6 us)
Async XLA Ops:
  6.5 172.3 %copy-start = (bf16[1,256,2048]{2,1,0:T(8,128)(2,1)S(1)}, bf16[1,256,2048]{2,1,0:T(8,128)(2,1)}, u32[]{:S(2)}) copy-start(bf16[1,256,2048]{2,1,0:T(8,128)(2,1)} %param.40) | copy-start | bytes 3145732
  8.6 2.2 copy-start.11
  8.7 2.7 copy-start.12
  8.7 2.7 copy-start.24
  8.8 16.9 %copy-start.8 = (f32[1,128,1,512]{1,3,2,0:T(8,128)}, f32[1,128,1,512]{1,3,2,0:T(8,128)S(1)}, u32[]{:S(2)}) copy-start(f32[1,128,1,512]{1,3,2,0:T(8,128)S(1)} %bitcast_add_fusion.1) | copy-start | bytes 786436
  10.1 1.6 copy-start.9
  10.1 1.6 copy-start.23
  10.8 11.2 %copy-start.2 = (f32[1,256,1,512]{1,3,2,0:T(8,128)}, f32[1,256,1,512]{1,3,2,0:T(8,128)S(1)}, u32[]{:S(2)}) copy-start(f32[1,256,1,512]{1,3,2,0:T(8,128)S(1)} %bitcast_add_fusion) | copy-start | bytes 1572868
  11.0 13.4 %copy-start.4 = (bf16[512,128]{0,1:T(8,128)(2,1)}, bf16[512,128]{0,1:T(8,128)(2,1)S(1)}, u32[]{:S(2)}) copy-start(bf16[512,128]{0,1:T(8,128)(2,1)S(1)} %copy.90) | copy-start | bytes 393220
  13.5 23.3 %all-to-all-start = ((bf16[16,390,64]{1,2,0:T(8,128)(2,1)}), bf16[16,390,64]{1,2,0:T(8,128)(2,1)S(1)}, u32[]{:S(2)}, u32[]{:S(2)}) async-start(bf16[16,390,64]{1,2,0:T(8,128)(2,1)} %broadcast_in_dim.64), calls=%async_computation | async-start | bytes 2097152 | tf_op jit(solution)/shard_map/all_to_all | solution.py:16
  20.9 16.2 %copy-start.19 = (pred[16]{0:T(512)(128)(4,1)}, pred[16]{0:T(512)(128)(4,1)S(1)}, u32[]{:S(2)}) copy-start(pred[16]{0:T(512)(128)(4,1)S(1)} %iota_compare_fusion.5) | copy-start | bytes 52
  22.0 3.7 %copy-start.13 = (bf16[512,128]{1,0:T(8,128)(2,1)S(1)}, bf16[512,128]{1,0:T(8,128)(2,1)}, u32[]{:S(2)}) copy-start(bf16[512,128]{1,0:T(8,128)(2,1)} %param.22) | copy-start | bytes 393220
  22.0 3.7 %copy-start.27 = (bf16[512,128]{1,0:T(8,128)(2,1)S(1)}, bf16[512,128]{1,0:T(8,128)(2,1)}, u32[]{:S(2)}) copy-start(bf16[512,128]{1,0:T(8,128)(2,1)} %param.21) | copy-start | bytes 393220
  39.9 5.4 %copy-start.5 = (bf16[512,128]{0,1:T(8,128)(2,1)S(1)}, bf16[512,128]{0,1:T(8,128)(2,1)}, u32[]{:S(2)}) copy-start(bf16[512,128]{0,1:T(8,128)(2,1)} %copy-done.4) | copy-start | bytes 393220
  39.9 6.1 %copy-start.20 = (pred[16]{0:T(512)(128)(4,1)S(1)}, pred[16]{0:T(512)(128)(4,1)}, u32[]{:S(2)}) copy-start(pred[16]{0:T(512)(128)(4,1)} %copy-done.19) | copy-start | bytes 52
  45.2 1.1 copy-start.3
  45.2 1.1 copy-start.10
  45.2 1.1 copy-start.26
  46.1 1.1 copy-start.6
  46.1 1.1 copy-start.21
  46.4 1.6 copy-start.7
  50.2 8.8 %copy-start.22 = (s32[32]{0:T(128)S(1)}, s32[32]{0:T(128)}, u32[]{:S(2)}) copy-start(s32[32]{0:T(128)} %param.41) | copy-start | bytes 388
  50.2 58.5 %copy-start.14 = (bf16[32,2048]{1,0:T(8,128)(2,1)S(1)}, bf16[32,2048]{1,0:T(8,128)(2,1)}, u32[]{:S(2)}) copy-start(bf16[32,2048]{1,0:T(8,128)(2,1)} %param.33) | copy-start | bytes 393220
  50.2 58.5 %copy-start.15 = (f32[2048]{0:T(1024)S(1)}, f32[2048]{0:T(1024)}, u32[]{:S(2)}) copy-start(f32[2048]{0:T(1024)} %param.34) | copy-start | bytes 24580
  50.2 58.8 %copy-start.18 = (f32[2048]{0:T(1024)S(1)}, f32[2048]{0:T(1024)}, u32[]{:S(2)}) copy-start(f32[2048]{0:T(1024)} %param.35) | copy-start | bytes 24580
  50.2 58.0 %all-to-all-start.1 = ((bf16[16,32,2048]{2,1,0:T(8,128)(2,1)}), bf16[16,32,2048]{2,1,0:T(8,128)(2,1)S(1)}, u32[]{:S(2)}, u32[]{:S(2)}) async-start(bf16[16,32,2048]{2,1,0:T(8,128)(2,1)} %bitcast.206), calls=%async_computation.1 | async-start | bytes 4194304 | tf_op jit(solution)/shard_map/all_to_all | solution.py:76
  58.9 100.4 %all-gather.2.cloned.1.call-start = ((), (), s32[]{:S(2)}) async-start(), calls=%async_computation.5 | async-start | bytes 3342336 | tf_op jit(solution)/shard_map/all_gather | solution.py:277
  165.8 8.8 %copy-start.16 = (bf16[2048,2]{0,1:T(2,128)(2,1)S(1)}, bf16[2048,2]{0,1:T(2,128)(2,1)}, u32[]{:S(2)}) copy-start(bf16[2048,2]{0,1:T(2,128)(2,1)} %param.37) | copy-start | bytes 24580
  174.6 3.0 copy-start.1
  174.7 3.1 %copy-start.25 = (bf16[1,2048,256]{2,1,0:T(8,128)(2,1)S(1)}, bf16[1,2048,256]{2,1,0:T(8,128)(2,1)}, u32[]{:S(2)}) copy-start(bf16[1,2048,256]{2,1,0:T(8,128)(2,1)} %param.38) | copy-start | bytes 3145732
  276.3 18.6 %copy-start.17 = (f32[2048]{0:T(1024)S(1)}, f32[2048]{0:T(1024)}, u32[]{:S(2)}) copy-start(f32[2048]{0:T(1024)} %param.36) | copy-start | bytes 24580
Sparse Core Ops, SparseCore 0:
  122.8 36.4 all-gather.1
where the time goes:
time: 306 us; the launch traced here: 302 us
  blocking collectives  104 us (34%)
  waiting for transfers between devices  95.4 us (31%)
  local copies, waits for them, and re-layouts  36.5 us (12%)
  matrix products  23.3 us (8%)
  starting transfers between devices  16.2 us (5%)
  between operations  14 us (5%)
  other arithmetic  12.7 us (4%)
    all_to_all x1, blocking collectives, summed_on_arrival(): lax.all_to_all(parts, axis, split_axis=0, concat_axis=0, tiled=True)  76.4 us
    all_to_all x1, waiting for transfers between devices, summed_on_arrival(): lax.all_to_all(parts, axis, split_axis=0, concat_axis=0, tiled=True)  48.9 us
    all_gather x1, waiting for transfers between devices, shards(): lax.all_gather(incoming, 'tp', axis=0, tiled=True)  36.6 us
    all_to_all x1, blocking collectives, shards(): lax.all_to_all(summed.astype(jnp.bfloat16), 'sp', split_axis=0, concat_ax...  15.4 us
    reshape x2, local copies, waits for them, and re-layouts, split_up(): return jnp.moveaxis(shard.reshape(*before, length, -1, *after), dim, 0)  13.8 us
    all_to_all x1, blocking collectives, shards(): lax.all_to_all(outgoing, 'sp', split_axis=0, concat_axis=0, tiled=True)  12.5 us
    all_to_all x1, waiting for transfers between devices, copy_for_each(): lax.all_to_all(jnp.broadcast_to(shard[None], (length, *shard.shape)), axi...  9.95 us
    reshape x1, local copies, waits for them, and re-layouts, expert_rows(): flat_rows = piece.reshape(-1, piece.shape[-1])  8.83 us
  transfers between devices with their start and end apart: 3, of which 3 were waited for; matrix products, arithmetic and copies ran while one was open for 2% of the time, Pallas kernels for 0%

commit v1 on v0

v1 whole, which is shorter than its diff:
```python
import functools

import jax
import jax.numpy as jnp
from jax import lax
from jax.experimental import pallas as pl
from jax.experimental.pallas import tpu as pltpu
from jax.sharding import PartitionSpec as P

EPSILON = 1e-06
NX, NY, NZ = 4, 4, 8
NS = NX * NY
D = 2048
KT = 384
TOK = 512
ROWS = 32
CAP = 3
SLOTS = NS * CAP
LINES = D // 128
HID = 256
FAR, NEAR = NZ // 2, NZ // 2 - 1
PLACE = {0: 0, 7: 1, 1: 2, 6: 3, 2: 4, 5: 5, 3: 6, 4: 7}
DCH, GCH = 2, 3
MESH = pl.DeviceIdType.MESH
F32, BF16 = jnp.float32, jnp.bfloat16


def dot(a, b):
    return jnp.dot(a, b, preferred_element_type=F32)


def dot_nt(a, b):
    return lax.dot_general(a, b, (((1,), (1,)), ((), ())), preferred_element_type=F32)


def dot_tn(a, b):
    return lax.dot_general(a, b, (((0,), (0,)), ((), ())), preferred_element_type=F32)


def sigmoid(v):
    return 1.0 / (1.0 + jnp.exp(-v))


def rms(v, gain):
    return v * lax.rsqrt(jnp.mean(v * v, axis=-1, keepdims=True) + EPSILON) * gain


def split3(v):
    high = v.astype(BF16)
    rest = v - high.astype(F32)
    mid = rest.astype(BF16)
    low = (rest - mid.astype(F32)).astype(BF16)
    return high, mid, low


def iota(shape, dim):
    return lax.broadcasted_iota(jnp.int32, shape, dim)


def kernel(
    qa_ref, fa_ref, ga_ref, qb_ref, fb_ref, gb_ref, v_ref, gate_ref, bias_ref, lane_ref,
    skip_ref, post_ref, pre_ref, postmix_ref, router_ref, cluster_ref,
    alpha_ref, beta_ref, sw_ref, ex_ref, co_ref,
    out_ref,
    key_s, ins_s, qd_s, kg_s, wk_s, intra_s, buf1, buf2, row_s, hd_s, hrecv, wproj, p_s,
    dsend, drecv, hmid_s, out_rt, x_rt, conv_s, x_s, part_s, swv, exv, cov, gsend, grecv, ret_rt, fin_rt,
    wsem, wssem, wrsem, s1s, s1r, s2s, s2r, hs, hr, dss, drs, dps, dpr, ags, agr, gss, grs, rts, rtr,
):
    s = lax.axis_index("sp")
    t = lax.axis_index("tp")
    y, x = s // NX, lax.rem(s, NX)
    z, c = t // 2, lax.rem(t, 2)
    way = 1 - 2 * c
    ahead = lax.rem(z + way + NZ, NZ) * 2 + c
    behind = lax.rem(z - way + NZ, NZ) * 2 + c
    sibling = z * 2 + 1 - c

    def remote(src, dst, ssem, rsem, sp, tp):
        return pltpu.make_async_remote_copy(
            src_ref=src, dst_ref=dst, send_sem=ssem, recv_sem=rsem,
            device_id=(sp, tp), device_id_type=MESH,
        )

    barrier = pltpu.get_barrier_semaphore()

    def greet(d, carry):
        pl.semaphore_signal(barrier, inc=1, device_id=(lax.rem(s + d, NS), t), device_id_type=MESH)
        return carry

    lax.fori_loop(1, NS, greet, 0)
    for peer in (ahead, behind, sibling):
        pl.semaphore_signal(barrier, inc=1, device_id=(s, peer), device_id_type=MESH)

    own_weights = [
        pltpu.make_async_copy(alpha_ref, wproj.at[0, pl.ds(0, 64)], wsem.at[0]),
        pltpu.make_async_copy(beta_ref, wproj.at[0, pl.ds(64, 64)], wsem.at[1]),
        pltpu.make_async_copy(sw_ref.at[0], swv.at[0], wsem.at[2]),
        pltpu.make_async_copy(ex_ref.at[0], exv.at[0], wsem.at[3]),
        pltpu.make_async_copy(co_ref.at[0], cov.at[0], wsem.at[4]),
    ]
    for copy in own_weights:
        copy.start()

    gap = jnp.concatenate([ga_ref[...], gb_ref[...]], axis=1)
    lower = jnp.where(iota((128, 128), 0) >= iota((128, 128), 1), 1.0, 0.0).astype(BF16)

    def decays(r, carry):
        rows = pl.ds(pl.multiple_of(r * 128, 128), 128)
        forget = jnp.concatenate([fa_ref[rows, :].astype(F32), fb_ref[rows, :].astype(F32)], axis=1)
        key = gap * sigmoid(-forget)
        left = jnp.broadcast_to(bias_ref[0:1, rows], (128, 128)).T
        right = jnp.broadcast_to(bias_ref[1:2, rows], (128, 128)).T
        logf = jnp.log1p(-key) + jnp.concatenate([left, right, right], axis=1)
        high, mid, low = split3(logf)
        inside = dot(lower, high) + dot(lower, mid) + dot(lower, low) + carry
        key_s[rows, :] = key
        ins_s[rows, :] = inside
        return inside[127:128, :]

    last = lax.fori_loop(0, TOK // 128, decays, jnp.zeros((1, KT), F32))

    def scaled(r, carry):
        rows = pl.ds(pl.multiple_of(r * 128, 128), 128)
        ask = jnp.concatenate([qa_ref[rows, :].astype(F32), qb_ref[rows, :].astype(F32)], axis=1)
        key = key_s[rows, :]
        inside = ins_s[rows, :]
        qd_s[rows, :] = (ask * sigmoid(ask) * jnp.exp(inside)).astype(BF16)
        kg_s[rows, :] = (key * jnp.exp(-inside)).astype(BF16)
        wk_s[rows, :] = (key * jnp.exp(last - inside)).astype(BF16)
        return carry

    lax.fori_loop(0, TOK // 128, scaled, 0)
    summed = dot_tn(v_ref[...], wk_s[...])
    state = jnp.concatenate([summed[0:64, 0:128], summed[64:128, 128:KT]], axis=1)

    def packed(buf, place, state, total):
        rows3 = iota((16, KT), 0)
        high, mid, low = (part.astype(F32) for part in split3(total))
        lines = jnp.where(rows3 == 0, high, jnp.where(rows3 == 1, mid, jnp.where(rows3 == 2, low, 0.0)))
        buf[place, 0:64, :] = state.astype(BF16)
        buf[place, 64:80, :] = lines.astype(BF16)

    def unpacked(buf, place):
        lines = buf[place, 64:80, :].astype(F32)
        return buf[place, 0:64, :].astype(F32), lines[0:1] + lines[1:2] + lines[2:3]

    packed(buf1, x, state, last)
    pl.semaphore_wait(barrier, NS + 2)

    def along_x(d):
        return remote(buf1.at[x], buf1.at[x], s1s.at[d], s1r.at[x], y * NX + lax.rem(x + d, NX), t)

    def from_x(d):
        there = lax.rem(x + d, NX)
        return remote(buf1.at[there], buf1.at[there], s1s.at[d], s1r.at[there], y * NX + there, t)

    for d in range(1, NX):
        along_x(d).start()

    shared = [
        (alpha_ref, wproj.at[1, pl.ds(0, 64)]), (beta_ref, wproj.at[1, pl.ds(64, 64)]),
        (sw_ref.at[0], swv.at[1]), (ex_ref.at[0], exv.at[1]), (co_ref.at[0], cov.at[1]),
    ]
    shared = [remote(a, b, wssem.at[k], wrsem.at[k], s, sibling) for k, (a, b) in enumerate(shared)]
    for copy in shared:
        copy.start()

    left_half = iota((256, 128), 1) < 64

    def intra(columns, first):
        for block in range(2):
            rows, width = slice(block * 256, block * 256 + 256), 256 * (block + 1)
            scores = dot_nt(qd_s[rows, columns], kg_s[0:width, columns])
            causal = iota((256, width), 0) + 256 * block >= iota((256, width), 1)
            scores = jnp.where(causal, scores, 0.0).astype(BF16)
            found = dot(scores, v_ref[0:width, :])
            intra_s[rows, :] = found if first else jnp.where(left_half, intra_s[rows, :], found)

    intra(slice(0, 128), True)

    for d in range(1, NX):
        from_x(d).wait_recv()
    sofar, gone = jnp.zeros((64, KT), F32), jnp.zeros((1, KT), F32)
    before, before_gone = sofar, gone
    for k in range(NX):
        before = jnp.where(x == k, sofar, before)
        before_gone = jnp.where(x == k, gone, before_gone)
        piece, total = unpacked(buf1, k)
        sofar = jnp.exp(total) * sofar + piece
        gone = gone + total
    packed(buf2, y, sofar, gone)
    row_s[...] = jnp.zeros_like(row_s)

    def along_y(d):
        return remote(buf2.at[y], buf2.at[y], s2s.at[d], s2r.at[y], (y + d) * NX + x, t)

    def from_y(k):
        return remote(buf2.at[k], buf2.at[k], s2s.at[0], s2r.at[k], k * NX + x, t)

    for d in range(1, NY):
        @pl.when(y + d < NY)
        def _():
            along_y(d).start()

    intra(slice(128, KT), False)

    for k in range(NY - 1):
        @pl.when(k < y)
        def _():
            from_y(k).wait_recv()
            piece, total = unpacked(buf2, k)
            row_s[...] = jnp.exp(total) * row_s[...] + piece

    carried = jnp.exp(before_gone) * row_s[...] + before
    is_left = iota((64, KT), 1) < 128
    carried = jnp.concatenate(
        [jnp.where(is_left, carried, 0.0), jnp.where(is_left, 0.0, carried)], axis=0
    ).astype(BF16)
    lane_gain = jnp.concatenate([lane_ref[...], lane_ref[...]], axis=1)
    left = iota((128, 128), 1) < 64
    for r in range(TOK // 128):
        rows = slice(r * 128, r * 128 + 128)
        raw = intra_s[rows, :] + dot_nt(qd_s[rows, :], carried)
        squares = raw * raw
        mean_a = jnp.sum(jnp.where(left, squares, 0.0), axis=1, keepdims=True) * (1.0 / 64)
        mean_b = jnp.sum(jnp.where(left, 0.0, squares), axis=1, keepdims=True) * (1.0 / 64)
        mean = jnp.where(left, mean_a, mean_b)
        head = raw * lax.rsqrt(mean + EPSILON) * lane_gain * sigmoid(gate_ref[rows, :].astype(F32))
        head = head.astype(BF16)
        for q in range(4):
            at = (2 * r + q // 2) * 32
            hd_s[q % 2, at : at + 32, :] = head[q * 32 : q * 32 + 32, :]

    swap = remote(hd_s.at[1 - c], hrecv, hs, hr, s, sibling)
    swap.start()
    for copy in own_weights[:2]:
        copy.wait()
    p_s[...] = dot(hd_s[c], wproj[0])
    for copy in shared[:2]:
        copy.wait_recv()
    swap.wait_recv()
    p_s[...] = p_s[...] + dot(hrecv[...], wproj[1])

    HALF = ROWS // DCH

    def ring_d(k, j):
        part = pl.ds(j * HALF, HALF)
        return remote(
            dsend.at[k, part], drecv.at[k, part], dss.at[k, j], drs.at[k, j], s,
            ahead if k < FAR else behind,
        )

    def send_d(k, j, first):
        place = FAR - k if k < FAR else -(NEAR - (k - FAR))
        target = lax.rem(z + way * place + NZ, NZ)
        rows = pl.ds(pl.multiple_of(target * ROWS + j * HALF, HALF), HALF)
        value = p_s[rows, :]
        if not first:
            ring_d(k - 1, j).wait_recv()
            value = value + drecv[k - 1, j * HALF : (j + 1) * HALF, :].astype(F32)
        dsend[k, j * HALF : (j + 1) * HALF, :] = value.astype(BF16)
        ring_d(k, j).start()

    for step in range(FAR):
        for j in range(DCH):
            send_d(step, j, step == 0)
            if step < NEAR:
                send_d(FAR + step, j, step == 0)
    mixed = p_s[pl.ds(pl.multiple_of(z * ROWS, ROWS), ROWS), :]
    for k in (FAR + NEAR - 1, FAR - 1):
        for j in range(DCH):
            ring_d(k, j).wait_recv()
        mixed = mixed + drecv[k].astype(F32)

    h_mid = (skip_ref[...].astype(F32) + rms(mixed, post_ref[...])).astype(BF16).astype(F32)
    hmid_s[...] = h_mid
    normed = rms(h_mid, pre_ref[...]).astype(BF16)

    group_row = jnp.broadcast_to(cluster_ref[...], (ROWS, ROWS))
    group_row = group_row.astype(F32)
    diagonal = iota((ROWS, ROWS), 0) == iota((ROWS, ROWS), 1)
    group_column = jnp.sum(jnp.where(diagonal, group_row, 0.0), axis=1, keepdims=True)
    same = jnp.where(group_row == group_column, 1.0, 0.0)
    earlier_row = iota((ROWS, ROWS), 0) < iota((ROWS, ROWS), 1)
    rank_row = jnp.sum(jnp.where(earlier_row, same, 0.0), axis=0, keepdims=True)
    earlier_column = iota((ROWS, ROWS), 1) < iota((ROWS, ROWS), 0)
    rank_column = jnp.sum(jnp.where(earlier_column, same, 0.0), axis=1, keepdims=True)
    slot_row = group_row[0:1, :] * CAP + rank_row
    slot_column = group_column * CAP + rank_column
    placing = jnp.where(
        iota((SLOTS, ROWS), 0).astype(F32) == slot_row, 1.0, 0.0
    ).astype(BF16)
    placed_back = jnp.where(
        iota((ROWS, SLOTS), 1).astype(F32) == slot_column, 1.0, 0.0
    ).astype(BF16)

    def to_lines(value):
        for i in range(LINES):
            conv_s[pl.ds(i, SLOTS, stride=LINES), :] = value[:, i * 128 : i * 128 + 128]
        return conv_s[...].astype(BF16)

    out_rt[...] = to_lines(dot(placing, normed))
    own = pl.ds(pl.multiple_of(s * (CAP * LINES), CAP * LINES), CAP * LINES)

    def lines_of(k):
        return pl.ds(pl.multiple_of(k * (CAP * LINES), CAP * LINES), CAP * LINES)

    def dispatch(d):
        there = lax.rem(s + d, NS)
        return remote(out_rt.at[lines_of(there)], x_rt.at[0, own], dps.at[d], dpr.at[s], there, t)

    def dispatched(d):
        there = lax.rem(s + d, NS)
        return remote(out_rt.at[own], x_rt.at[0, lines_of(there)], dps.at[d], dpr.at[there], there, t)

    def each(action):
        def body(d, carry):
            action(d)
            return carry

        lax.fori_loop(1, NS, body, 0)

    each(lambda d: dispatch(d).start())
    x_rt[0, own, :] = out_rt[own, :]

    for copy in own_weights[2:]:
        copy.wait()
    router = router_ref[...].astype(F32)
    router_rows = iota((16, D), 0)
    router = jnp.where(
        router_rows == 0, router[0:1], jnp.where(router_rows == 1, router[1:2], 0.0)
    ).astype(BF16)
    member = z // (NZ // 2)

    def ring_g(k, j):
        source = (NZ - k) % NZ if k < FAR else k - FAR
        target = (source + NZ - 1) % NZ if k < FAR else source + 1
        part = pl.ds(j * (SLOTS // GCH * LINES), SLOTS // GCH * LINES)
        return remote(
            x_rt.at[source, part], x_rt.at[target, part], ags.at[k, j], agr.at[k, j], s,
            ahead if k < FAR else behind,
        )

    def to_rows(place):
        conv_s[...] = x_rt[place].astype(F32)
        at = PLACE[place] * SLOTS
        for i in range(LINES):
            x_s[at : at + SLOTS, i * 128 : i * 128 + 128] = conv_s[
                pl.ds(i, SLOTS, stride=LINES), :
            ].astype(BF16)

    def compute(places):
        for place in places:
            to_rows(place)
        at, size = PLACE[places[0]] * SLOTS, SLOTS * len(places)
        rows = x_s[at : at + size, :]
        scores = sigmoid(dot_nt(rows, router))
        first, second = scores[:, 0:1], scores[:, 1:2]
        weight = jnp.where(member == 0, first, second) / (first + second)
        total = None
        for u in range(2):
            gate = dot(rows, swv[u])
            hidden = (gate * sigmoid(gate) * dot(rows, exv[u])).astype(BF16)
            term = dot(hidden, cov[u])
            total = term if total is None else total + term
        part_s[at : at + size, :] = total * weight

    each(lambda d: dispatched(d).wait_recv())
    for j in range(GCH):
        ring_g(0, j).start()
        ring_g(FAR, j).start()
    for copy in shared[2:]:
        copy.wait_recv()
    compute((0,))
    for k in range(FAR):
        for j in range(GCH):
            ring_g(k, j).wait_recv()
            if k + 1 < FAR:
                ring_g(k + 1, j).start()
            if k < NEAR:
                ring_g(FAR + k, j).wait_recv()
                if k + 1 < NEAR:
                    ring_g(FAR + k + 1, j).start()
        compute((NZ - 1 - k, k + 1) if k < NEAR else (NZ - 1 - k,))

    PART = SLOTS // GCH

    def ring_p(k, j):
        part = pl.ds(j * PART, PART)
        return remote(
            gsend.at[k, part], grecv.at[k, part], gss.at[k, j], grs.at[k, j], s,
            ahead if k < FAR else behind,
        )

    def send_p(k, j, first):
        place = PLACE[FAR - k if k < FAR else NZ - (NEAR - (k - FAR))]
        value = part_s[place * SLOTS + j * PART : place * SLOTS + (j + 1) * PART, :]
        if not first:
            ring_p(k - 1, j).wait_recv()
            value = value + grecv[k - 1, j * PART : (j + 1) * PART, :].astype(F32)
        gsend[k, j * PART : (j + 1) * PART, :] = value.astype(BF16)
        ring_p(k, j).start()

    for step in range(FAR):
        for j in range(GCH):
            send_p(step, j, step == 0)
            if step < NEAR:
                send_p(FAR + step, j, step == 0)
    final = part_s[0:SLOTS, :]
    for k in (FAR + NEAR - 1, FAR - 1):
        for j in range(GCH):
            ring_p(k, j).wait_recv()
        final = final + grecv[k].astype(F32)

    fin_rt[...] = to_lines(final)

    def give(d):
        there = lax.rem(s + d, NS)
        return remote(fin_rt.at[lines_of(there)], ret_rt.at[own], rts.at[d], rtr.at[s], there, t)

    def given(d):
        there = lax.rem(s + d, NS)
        return remote(fin_rt.at[own], ret_rt.at[lines_of(there)], rts.at[d], rtr.at[there], there, t)

    each(lambda d: give(d).start())
    ret_rt[own, :] = fin_rt[own, :]

    for d in range(1, NX):
        along_x(d).wait_send()
    for d in range(1, NY):
        @pl.when(y + d < NY)
        def _():
            along_y(d).wait_send()
    for copy in shared:
        copy.wait_send()
    swap.wait_send()
    for k in range(FAR + NEAR):
        for j in range(DCH):
            ring_d(k, j).wait_send()
        for j in range(GCH):
            ring_g(k, j).wait_send()
            ring_p(k, j).wait_send()
    each(lambda d: dispatch(d).wait_send())

    each(lambda d: given(d).wait_recv())
    conv_s[...] = ret_rt[...].astype(F32)
    for i in range(LINES):
        x_s[0:SLOTS, i * 128 : i * 128 + 128] = conv_s[pl.ds(i, SLOTS, stride=LINES), :].astype(BF16)
    routed = dot(placed_back, x_s[0:SLOTS, :])
    out_ref[...] = (hmid_s[...] + rms(routed, postmix_ref[...])).astype(BF16)
    each(lambda d: give(d).wait_send())


def shards(
    ask_left, keep_left, gap_left, ask_right, keep_right, gap_right, payload, switch_logits,
    keep_bias, lanewise, alpha, beta, skip, post, pre, postmix, router, switch, expansion,
    contraction, cluster,
):
    vmem = pl.BlockSpec(memory_space=pltpu.VMEM)
    hbm = pl.BlockSpec(memory_space=pl.ANY)
    ring = FAR + NEAR
    dma, lines = pltpu.SemaphoreType.DMA, SLOTS * LINES
    return pl.pallas_call(
        kernel,
        out_shape=jax.ShapeDtypeStruct((ROWS, D), BF16),
        in_specs=[vmem] * 16 + [hbm] * 5,
        out_specs=vmem,
        scratch_shapes=[
            pltpu.VMEM((TOK, KT), F32),
            pltpu.VMEM((TOK, KT), F32),
            pltpu.VMEM((TOK, KT), BF16),
            pltpu.VMEM((TOK, KT), BF16),
            pltpu.VMEM((TOK, KT), BF16),
            pltpu.VMEM((TOK, 128), F32),
            pltpu.VMEM((NX, 80, KT), BF16),
            pltpu.VMEM((NY, 80, KT), BF16),
            pltpu.VMEM((64, KT), F32),
            pltpu.VMEM((2, TOK // 2, 128), BF16),
            pltpu.VMEM((TOK // 2, 128), BF16),
            pltpu.VMEM((2, 128, D), BF16),
            pltpu.VMEM((TOK // 2, D), F32),
            pltpu.VMEM((ring, ROWS, D), BF16),
            pltpu.VMEM((ring, ROWS, D), BF16),
            pltpu.VMEM((ROWS, D), F32),
            pltpu.VMEM((lines, 128), BF16),
            pltpu.VMEM((NZ, lines, 128), BF16),
            pltpu.VMEM((lines, 128), F32),
            pltpu.VMEM((NZ * SLOTS, D), BF16),
            pltpu.VMEM((NZ * SLOTS, D), F32),
            pltpu.VMEM((2, D, HID), BF16),
            pltpu.VMEM((2, D, HID), BF16),
            pltpu.VMEM((2, HID, D), BF16),
            pltpu.VMEM((ring, SLOTS, D), BF16),
            pltpu.VMEM((ring, SLOTS, D), BF16),
            pltpu.VMEM((lines, 128), BF16),
            pltpu.VMEM((lines, 128), BF16),
            dma((5,)), dma((5,)), dma((5,)),
            dma((NX,)), dma((NX,)), dma((NY,)), dma((NY,)),
            dma, dma,
            dma((ring, DCH)), dma((ring, DCH)),
            dma((NS,)), dma((NS,)),
            dma((ring, GCH)), dma((ring, GCH)),
            dma((ring, GCH)), dma((ring, GCH)),
            dma((NS,)), dma((NS,)),
        ],
        compiler_params=pltpu.CompilerParams(
            collective_id=0, has_side_effects=True, vmem_limit_bytes=56 * 1024 * 1024
        ),
    )(
        ask_left, keep_left, gap_left.reshape(1, -1), ask_right, keep_right,
        gap_right.reshape(1, -1), payload, switch_logits, keep_bias.T, lanewise.reshape(1, -1),
        skip, post.reshape(1, -1), pre.reshape(1, -1), postmix.reshape(1, -1), router.T,
        cluster.reshape(1, -1), alpha, beta, switch, expansion, contraction,
    )


def solution(mesh):
    placed = (
        P("sp", "tp"),
        P("sp", "tp"),
        P("tp"),
        P("sp", "tp"),
        P("sp", "tp"),
        P("tp"),
        P("sp", "tp"),
        P("sp", "tp"),
        P("sp", "tp"),
        P(),
        P("tp", None),
        P("tp", None),
        P(("sp", "tp"), None),
        P(),
        P(),
        P(),
        P(None, "sp"),
        P("sp", None, "tp"),
        P("sp", None, "tp"),
        P("sp", "tp", None),
        P(("sp", "tp")),
    )
    return jax.shard_map(
        shards, mesh=mesh, in_specs=placed, out_specs=P(("sp", "tp"), None), check_vma=False
    )
```

time: 306 us -> 89.8 us (0.29); the launches traced: 302 us -> 89.6 us
  blocking collectives: 104 us -> 0 us
  waiting for transfers between devices: 95.4 us -> 0 us
  Pallas kernels: 0 us -> 88 us
  local copies, waits for them, and re-layouts: 36.5 us -> 1.57 us
  matrix products: 23.3 us -> 0 us
  starting transfers between devices: 16.2 us -> 0 us
  between operations: 14 us -> 0.01 us
  other arithmetic: 12.7 us -> 0 us
    all_to_all x3 -> x0, blocking collectives: 104 us -> none  [the longest x1 76.4 us: summed_on_arrival(): lax.all_to_all(parts, axis, split_axis=0, concat_axis=0, tiled=True)]
    pallas_call x0 -> x1, Pallas kernels: none -> 88 us  [shards(): pl.pallas_call(kernel, out_shape=jax.ShapeDtypeStruct((ROWS, D), BF16), i...]
    all_to_all x2 -> x0, waiting for transfers between devices: 58.8 us -> none  [the longest x1 48.9 us: summed_on_arrival(): lax.all_to_all(parts, axis, split_axis=0, concat_axis=0, tiled=True)]
    all_gather x1 -> x0, waiting for transfers between devices: 36.6 us -> none  [shards(): lax.all_gather(incoming, 'tp', axis=0, tiled=True)]
    dot_general x15 -> x0, matrix products: 23.3 us -> none  [the longest x1 7.17 us: expert_rows(): jnp.dot(hidden, contraction_matrix[0], preferred_element_type=jnp.float32)]
    reshape x5 -> x0, local copies, waits for them, and re-layouts: 22.9 us -> none  [the longest x2 13.8 us: split_up(): return jnp.moveaxis(shard.reshape(*before, length, -1, *after), dim, 0)]
    all_to_all x2 -> x0, starting transfers between devices: 16.2 us -> none  [the longest x1 8.73 us: summed_on_arrival(): lax.all_to_all(parts, axis, split_axis=0, concat_axis=0, tiled=True)]
    all_gather x1 -> x0, local copies, waits for them, and re-layouts: 6.51 us -> none  [shards(): lax.all_gather(incoming, 'tp', axis=0, tiled=True)]
  transfers between devices with their start and end apart: 3 -> 0, of which waited for: 3 -> 0; matrix products, arithmetic and copies ran while one was open for 2% -> 0% of each run, Pallas kernels for 0% -> 0%
where the time goes in v1:
time: 89.8 us; the launch traced here: 89.6 us
  Pallas kernels  88 us (98%)
  local copies, waits for them, and re-layouts  1.57 us (2%)
    pallas_call x1, Pallas kernels, shards(): pl.pallas_call(kernel, out_shape=jax.ShapeDtypeStruct((ROWS, D), BF16), i...  88 us

profile of v1, /device:TPU:2, one launch (start us, length us, event | category | flops | bytes accessed | tf_op | source)
XLA Modules:
  0.0 89.6 jit_solution(1650663075345867177)
XLA Ops:
  0.0 88.0 %shard_map.199 = bf16[32,2048]{1,0:T(8,128)(2,1)} custom-call(bf16[512,128]{1,0:T(8,128)(2,1)} %qa_ref.1, bf16[512,128]{1,0:T(8,128)(2,1)} %fa_ref.1, f32[1,128]{1,0:T(1,128)} %bitcast.15, bf16[512,256]{1,0:T(8,128)(2,1)} %qb_ref.1, bf16[512,256]{1,0:T(8,128)(2,1)} %fb_ref.1, f32[1,256]{1,0:T(1,128)} %bitcast.14, bf16[512,128]{1,0:T(8,128)(2,1)} %v_ref.1, ...), custom_call_target="tpu_custom_call" | custom-call | tf_op jit(solution)/shard_map/pallas_call | solution.py:463
  88.0 1.6 %copy.23 = bf16[32,2048]{1,0:T(8,128)(2,1)} copy(bf16[32,2048]{1,0:T(8,128)(2,1)} %shard_map.199) | data formatting | bytes 262144

commit v2 on v1

v2 whole, which is shorter than its diff:
```python
import functools

import jax
import jax.numpy as jnp
from jax import lax
from jax.experimental import pallas as pl
from jax.experimental.pallas import tpu as pltpu
from jax.sharding import PartitionSpec as P

EPSILON = 1e-06
NX, NY, NZ = 4, 4, 8
NS = NX * NY
D = 2048
KT = 384
TOK = 512
ROWS = 32
CAP = 3
SLOTS = NS * CAP
LINES = D // 128
HID = 256
FAR, NEAR = NZ // 2, NZ // 2 - 1
PLACE = {0: 0, 7: 1, 1: 2, 6: 3, 2: 4, 5: 5, 3: 6, 4: 7}
PITCH = 24
OFFSETS = sorted(
    ((dy, dx) for dy in range(NY) for dx in range(NX)),
    key=lambda o: min(o[0], NY - o[0]) + min(o[1], NX - o[1]),
)
DCH, GCH, ZCH, ACH = 4, 6, 4, 4
MESH = pl.DeviceIdType.MESH
F32, BF16 = jnp.float32, jnp.bfloat16


def dot(a, b):
    return jnp.dot(a, b, preferred_element_type=F32)


def dot_nt(a, b):
    return lax.dot_general(a, b, (((1,), (1,)), ((), ())), preferred_element_type=F32)


def dot_tn(a, b):
    return lax.dot_general(a, b, (((0,), (0,)), ((), ())), preferred_element_type=F32)


def sigmoid(v):
    return 1.0 / (1.0 + jnp.exp(-v))


def rms(v, gain):
    return v * lax.rsqrt(jnp.mean(v * v, axis=-1, keepdims=True) + EPSILON) * gain


def split3(v):
    high = v.astype(BF16)
    rest = v - high.astype(F32)
    mid = rest.astype(BF16)
    low = (rest - mid.astype(F32)).astype(BF16)
    return high, mid, low


def iota(shape, dim):
    return lax.broadcasted_iota(jnp.int32, shape, dim)


def kernel(
    fa_hbm, fb_hbm, ga_hbm, gb_hbm, bias_hbm, cluster_hbm, qa_hbm, qb_hbm, v_hbm,
    gate_hbm, lane_hbm, skip_hbm, post_hbm, pre_hbm, postmix_hbm, router_hbm,
    alpha_ref, beta_ref, sw_ref, ex_ref, co_ref,
    out_ref,
    fa_ref, fb_ref, ga_ref, gb_ref, bias_ref, cluster_ref, qa_ref, qb_ref, v_ref,
    gate_ref, lane_ref, skip_ref, post_ref, pre_ref, postmix_ref, router_ref, insem,
    key_s, ins_s, qd_s, kg_s, wk_s, intra_s, buf1, buf2, row_s, hd_s, hrecv, wproj, p_s,
    dsend, drecv, hmid_s, out_rt, x_rt, conv_s, x_s, part_s, swv, exv, cov, gsend, grecv, ret_rt, fin_rt,
    clus_s, place_s, unplace_s, nz_s, qz_s,
    cls, clr, zos, zor, zis, zir, xir,
    wsem, wssem, wrsem, s1s, s1r, s2s, s2r, hs, hr, dss, drs, ags, agr, gss, grs,
):
    s = lax.axis_index("sp")
    t = lax.axis_index("tp")
    y, x = s // NX, lax.rem(s, NX)
    z, c = t // 2, lax.rem(t, 2)
    way = 1 - 2 * c
    ahead = lax.rem(z + way + NZ, NZ) * 2 + c
    behind = lax.rem(z - way + NZ, NZ) * 2 + c
    sibling = z * 2 + 1 - c

    def remote(src, dst, ssem, rsem, sp, tp):
        return pltpu.make_async_remote_copy(
            src_ref=src, dst_ref=dst, send_sem=ssem, recv_sem=rsem,
            device_id=(sp, tp), device_id_type=MESH,
        )

    barrier = pltpu.get_barrier_semaphore()

    def greet(d, carry):
        pl.semaphore_signal(barrier, inc=1, device_id=(lax.rem(s + d, NS), t), device_id_type=MESH)
        return carry

    lax.fori_loop(1, NS, greet, 0)

    def greet_z(d, carry):
        peer = lax.rem(z + d, NZ) * 2 + c
        pl.semaphore_signal(barrier, inc=1, device_id=(s, peer), device_id_type=MESH)
        return carry

    lax.fori_loop(1, NZ, greet_z, 0)
    pl.semaphore_signal(barrier, inc=1, device_id=(s, sibling), device_id_type=MESH)

    inputs = [
        pltpu.make_async_copy(a, b, insem.at[k])
        for k, (a, b) in enumerate(
            [
                (fa_hbm, fa_ref), (fb_hbm, fb_ref), (ga_hbm, ga_ref), (gb_hbm, gb_ref),
                (bias_hbm, bias_ref), (cluster_hbm, cluster_ref), (qa_hbm, qa_ref),
                (qb_hbm, qb_ref), (v_hbm, v_ref), (gate_hbm, gate_ref), (lane_hbm, lane_ref),
                (skip_hbm, skip_ref), (post_hbm, post_ref), (pre_hbm, pre_ref),
                (postmix_hbm, postmix_ref), (router_hbm, router_ref),
            ]
        )
    ]
    for copy in inputs:
        copy.start()
    own_weights = [
        pltpu.make_async_copy(alpha_ref, wproj.at[0, pl.ds(0, 64)], wsem.at[0]),
        pltpu.make_async_copy(beta_ref, wproj.at[0, pl.ds(64, 64)], wsem.at[1]),
        pltpu.make_async_copy(sw_ref.at[0], swv.at[0], wsem.at[2]),
        pltpu.make_async_copy(ex_ref.at[0], exv.at[0], wsem.at[3]),
        pltpu.make_async_copy(co_ref.at[0], cov.at[0], wsem.at[4]),
    ]
    for copy in own_weights:
        copy.start()

    for copy in inputs[:6]:
        copy.wait()
    gap = jnp.concatenate([ga_ref[...], gb_ref[...]], axis=1)
    lower = jnp.where(iota((128, 128), 0) >= iota((128, 128), 1), 1.0, 0.0).astype(BF16)

    def decays(r, carry):
        rows = pl.ds(pl.multiple_of(r * 128, 128), 128)
        forget = jnp.concatenate([fa_ref[rows, :].astype(F32), fb_ref[rows, :].astype(F32)], axis=1)
        key = gap * sigmoid(-forget)
        left = jnp.broadcast_to(bias_ref[0:1, rows], (128, 128)).T
        right = jnp.broadcast_to(bias_ref[1:2, rows], (128, 128)).T
        logf = jnp.log1p(-key) + jnp.concatenate([left, right, right], axis=1)
        high, mid, low = split3(logf)
        inside = dot(lower, high) + dot(lower, mid) + dot(lower, low) + carry
        key_s[rows, :] = key
        ins_s[rows, :] = inside
        return inside[127:128, :]

    last = lax.fori_loop(0, TOK // 128, decays, jnp.zeros((1, KT), F32))

    def scaled(r, carry):
        rows = pl.ds(pl.multiple_of(r * 128, 128), 128)
        ask = jnp.concatenate([qa_ref[rows, :].astype(F32), qb_ref[rows, :].astype(F32)], axis=1)
        key = key_s[rows, :]
        inside = ins_s[rows, :]
        qd_s[rows, :] = (ask * sigmoid(ask) * jnp.exp(inside)).astype(BF16)
        kg_s[rows, :] = (key * jnp.exp(-inside)).astype(BF16)
        wk_s[rows, :] = (key * jnp.exp(last - inside)).astype(BF16)
        return carry

    for copy in inputs[6:9]:
        copy.wait()
    lax.fori_loop(0, TOK // 128, scaled, 0)
    summed = dot_tn(v_ref[...], wk_s[...])
    state = jnp.concatenate([summed[0:64, 0:128], summed[64:128, 128:KT]], axis=1)

    def packed(buf, place, state, total):
        rows3 = iota((8, KT), 0)
        high, mid, low = (part.astype(F32) for part in split3(total))
        lines = jnp.where(rows3 == 0, high, jnp.where(rows3 == 1, mid, jnp.where(rows3 == 2, low, 0.0)))
        buf[place, 0:64, :] = state.astype(BF16)
        buf[place, 64:72, :] = lines.astype(BF16)

    def unpacked(buf, place):
        lines = buf[place, 64:72, :].astype(F32)
        return buf[place, 0:64, :].astype(F32), lines[0:1] + lines[1:2] + lines[2:3]

    packed(buf1, x, state, last)
    clus_s[z] = jnp.zeros((8, 128), F32)
    clus_s[z, :, 0:ROWS] = jnp.broadcast_to(cluster_ref[...].astype(F32), (8, ROWS))
    pl.semaphore_wait(barrier, NS - 1 + NZ)

    def along_x(d):
        return remote(buf1.at[x], buf1.at[x], s1s, s1r.at[x], y * NX + lax.rem(x + d, NX), t)

    def from_x(d):
        there = lax.rem(x + d, NX)
        return remote(buf1.at[there], buf1.at[there], s1s, s1r.at[there], y * NX + there, t)

    for d in (2, 1, 3):
        along_x(d).start()

    shared = [
        (alpha_ref, wproj.at[1, pl.ds(0, 64)]), (beta_ref, wproj.at[1, pl.ds(64, 64)]),
        (sw_ref.at[0], swv.at[1]), (ex_ref.at[0], exv.at[1]), (co_ref.at[0], cov.at[1]),
    ]
    shared = [remote(a, b, wssem.at[k], wrsem.at[k], s, sibling) for k, (a, b) in enumerate(shared)]
    for copy in shared[:4]:
        copy.start()

    def share_groups(d):
        return remote(
            clus_s.at[z], clus_s.at[z], cls, clr, s, lax.rem(z + d, NZ) * 2 + c
        )

    def shared_groups():
        most = pl.ds(0, NZ - 1)
        return remote(clus_s.at[most], clus_s.at[most], cls, clr, s, ahead)

    def each(action, count=NS):
        def body(d, carry):
            action(d)
            return carry

        lax.fori_loop(1, count, body, 0)

    each(lambda d: share_groups(d).start(), NZ)
    left_half = iota((256, 128), 1) < 64

    def intra(columns, first):
        for block in range(2):
            rows, width = slice(block * 256, block * 256 + 256), 256 * (block + 1)
            scores = dot_nt(qd_s[rows, columns], kg_s[0:width, columns])
            causal = iota((256, width), 0) + 256 * block >= iota((256, width), 1)
            scores = jnp.where(causal, scores, 0.0).astype(BF16)
            found = dot(scores, v_ref[0:width, :])
            intra_s[rows, :] = found if first else jnp.where(left_half, intra_s[rows, :], found)

    for copy in inputs[9:]:
        copy.wait()
    intra(slice(0, 128), True)

    for d in range(1, NX):
        from_x(d).wait_recv()
    sofar, gone = jnp.zeros((64, KT), F32), jnp.zeros((1, KT), F32)
    before, before_gone = sofar, gone
    for k in range(NX):
        before = jnp.where(x == k, sofar, before)
        before_gone = jnp.where(x == k, gone, before_gone)
        piece, total = unpacked(buf1, k)
        sofar = jnp.exp(total) * sofar + piece
        gone = gone + total
    packed(buf2, y, sofar, gone)
    row_s[...] = jnp.zeros_like(row_s)

    def along_y(d):
        return remote(buf2.at[y], buf2.at[y], s2s.at[d], s2r.at[y], (y + d) * NX + x, t)

    def from_y(k):
        return remote(buf2.at[k], buf2.at[k], s2s.at[0], s2r.at[k], k * NX + x, t)

    for d in range(1, NY):
        @pl.when(y + d < NY)
        def _():
            along_y(d).start()

    intra(slice(128, KT), False)

    for k in range(NY - 1):
        @pl.when(k < y)
        def _():
            from_y(k).wait_recv()
            piece, total = unpacked(buf2, k)
            row_s[...] = jnp.exp(total) * row_s[...] + piece

    carried = jnp.exp(before_gone) * row_s[...] + before
    is_left = iota((64, KT), 1) < 128
    carried = jnp.concatenate(
        [jnp.where(is_left, carried, 0.0), jnp.where(is_left, 0.0, carried)], axis=0
    ).astype(BF16)
    lane_gain = jnp.concatenate([lane_ref[...], lane_ref[...]], axis=1)
    left = iota((128, 128), 1) < 64
    for r in range(TOK // 128):
        rows = slice(r * 128, r * 128 + 128)
        raw = intra_s[rows, :] + dot_nt(qd_s[rows, :], carried)
        squares = raw * raw
        mean_a = jnp.sum(jnp.where(left, squares, 0.0), axis=1, keepdims=True) * (1.0 / 64)
        mean_b = jnp.sum(jnp.where(left, 0.0, squares), axis=1, keepdims=True) * (1.0 / 64)
        mean = jnp.where(left, mean_a, mean_b)
        head = raw * lax.rsqrt(mean + EPSILON) * lane_gain * sigmoid(gate_ref[rows, :].astype(F32))
        head = head.astype(BF16)
        for q in range(4):
            at = (2 * r + q // 2) * 32
            hd_s[q % 2, at : at + 32, :] = head[q * 32 : q * 32 + 32, :]

    swap = remote(hd_s.at[1 - c], hrecv, hs, hr, s, sibling)
    swap.start()
    for copy in own_weights[:2]:
        copy.wait()
    p_s[...] = dot(hd_s[c], wproj[0])
    for copy in shared[:2]:
        copy.wait_recv()
    swap.wait_recv()
    p_s[...] = p_s[...] + dot(hrecv[...], wproj[1])

    HALF = ROWS // DCH

    def ring_d(k, j):
        part = pl.ds(j * HALF, HALF)
        return remote(
            dsend.at[k, part], drecv.at[k, part], dss, drs.at[k, j], s,
            ahead if k < FAR else behind,
        )

    def send_d(k, j, first):
        place = FAR - k if k < FAR else -(NEAR - (k - FAR))
        target = lax.rem(z + way * place + NZ, NZ)
        rows = pl.ds(pl.multiple_of(target * ROWS + j * HALF, HALF), HALF)
        value = p_s[rows, :]
        if not first:
            ring_d(k - 1, j).wait_recv()
            value = value + drecv[k - 1, j * HALF : (j + 1) * HALF, :].astype(F32)
        dsend[k, j * HALF : (j + 1) * HALF, :] = value.astype(BF16)
        ring_d(k, j).start()

    def slots_of(r, carry):
        there = lax.rem(z + way * r + NZ, NZ)
        group_row = jnp.broadcast_to(clus_s[there, 0:1, 0:ROWS], (ROWS, ROWS))
        diagonal = iota((ROWS, ROWS), 0) == iota((ROWS, ROWS), 1)
        group_column = jnp.sum(jnp.where(diagonal, group_row, 0.0), axis=1, keepdims=True)
        same = jnp.where(group_row == group_column, 1.0, 0.0)
        earlier_row = iota((ROWS, ROWS), 0) < iota((ROWS, ROWS), 1)
        rank_row = jnp.sum(jnp.where(earlier_row, same, 0.0), axis=0, keepdims=True)
        earlier_column = iota((ROWS, ROWS), 1) < iota((ROWS, ROWS), 0)
        rank_column = jnp.sum(jnp.where(earlier_column, same, 0.0), axis=1, keepdims=True)
        slot_row = group_row[0:1, :] * CAP + rank_row
        slot_column = group_column * CAP + rank_column
        place_s[r] = jnp.where(
            iota((SLOTS, ROWS), 0).astype(F32) == slot_row, 1.0, 0.0
        ).astype(BF16)
        unplace_s[r] = jnp.where(
            iota((ROWS, SLOTS), 1).astype(F32) == slot_column, 1.0, 0.0
        ).astype(BF16)
        return carry

    for step in range(FAR):
        for j in range(DCH):
            send_d(step, j, step == 0)
            if step < NEAR:
                send_d(FAR + step, j, step == 0)
        if step == 0:
            shared[4].start()
            shared_groups().wait_recv()
            lax.fori_loop(0, NZ, slots_of, 0)
    mixed = p_s[pl.ds(pl.multiple_of(z * ROWS, ROWS), ROWS), :]
    for k in (FAR + NEAR - 1, FAR - 1):
        for j in range(DCH):
            ring_d(k, j).wait_recv()
        mixed = mixed + drecv[k].astype(F32)

    h_mid = (skip_ref[...].astype(F32) + rms(mixed, post_ref[...])).astype(BF16).astype(F32)
    hmid_s[...] = h_mid
    nz_s[0] = rms(h_mid, pre_ref[...]).astype(BF16)

    lines3 = conv_s.reshape(SLOTS, PITCH, 128)
    own = pl.ds(s * CAP, CAP)

    def slots_for(k):
        return pl.ds(k * CAP, CAP)

    def to_lines(value):
        for i in range(LINES):
            conv_s[pl.ds(i, SLOTS, stride=PITCH), :] = value[:, i * 128 : i * 128 + 128]
        return lines3[:, 0:LINES, :].astype(BF16)

    def from_lines(value, at):
        lines3[:, 0:LINES, :] = value.astype(F32)
        for i in range(LINES):
            x_s[at : at + SLOTS, i * 128 : i * 128 + 128] = conv_s[
                pl.ds(i, SLOTS, stride=PITCH), :
            ].astype(BF16)

    def at_offset(dy, dx):
        return lax.rem(y + dy, NY) * NX + lax.rem(x + dx, NX)

    def far_first(action):
        middle = 2 * NX + 2

        def body(i, carry):
            i = i + jnp.where(i >= middle, 1, 0)
            action(at_offset(lax.rem(2 + i // NX, NY), lax.rem(2 + lax.rem(i, NX), NX)))
            return carry

        lax.fori_loop(0, NS - 1, body, 0)

    def all_but_own(src, dst, r, ssem, rsem):
        most = pl.ds(0, SLOTS - CAP)
        return remote(src.at[r, most], dst.at[r, most], ssem, rsem, lax.rem(s + 1, NS), t)

    def scatter(src, dst, r, ssem, rsem):
        far_first(
            lambda there: remote(
                src.at[r, slots_for(there)], dst.at[r, own], ssem, rsem, there, t
            ).start()
        )
        dst[r, own] = src[r, own]

    def near_slots(p):
        return pl.ds(p * CAP, CAP)

    def scatter_in(src, dst):
        for dy, dx in reversed(OFFSETS[1:]):
            there = at_offset(dy, dx)
            p = OFFSETS.index(((-dy) % NY, (-dx) % NX))
            remote(
                src.at[0, slots_for(there)], dst.at[0, near_slots(p)], zos, xir.at[p // (NS // ACH)],
                there, t,
            ).start()
        dst[0, 0:CAP] = src[0, own]

    def scattered_in(src, dst, q):
        first = 1 if q == 0 else q * (NS // ACH)
        part = pl.ds(first * CAP, ((q + 1) * (NS // ACH) - first) * CAP)
        return remote(src.at[0, part], dst.at[0, part], zos, xir.at[q], lax.rem(s + 1, NS), t)

    def scatter_back(src, dst, r, ssem, rsem):
        for p in range(NS - 1, 0, -1):
            there = at_offset(*OFFSETS[p])
            remote(src.at[r, near_slots(p)], dst.at[r, own], ssem, rsem, there, t).start()
        dst[r, own] = src[r, 0:CAP]

    def returned(r):
        all_but_own(fin_rt, ret_rt, r, zis, zir.at[r]).wait_recv()
        at = PLACE[r] * SLOTS
        from_lines(ret_rt[r], at)
        return dot(unplace_s[r], x_s[at : at + SLOTS, :])

    for copy in own_weights[2:]:
        copy.wait()
    router = router_ref[...].astype(F32)
    router_rows = iota((16, D), 0)
    router = jnp.where(
        router_rows == 0, router[0:1], jnp.where(router_rows == 1, router[1:2], 0.0)
    ).astype(BF16)
    member = z // (NZ // 2)

    def part_of(r):
        return part_s[PLACE[r] * SLOTS : PLACE[r] * SLOTS + SLOTS, :]

    def compute(places):
        for place in places:
            from_lines(x_rt[place], PLACE[place] * SLOTS)
        at, size = PLACE[places[0]] * SLOTS, SLOTS * len(places)
        rows = x_s[at : at + size, :]
        scores = sigmoid(dot_nt(rows, router))
        first, second = scores[:, 0:1], scores[:, 1:2]
        weight = jnp.where(member == 0, first, second) / (first + second)
        total = None
        for u in range(2):
            gate = dot(rows, swv[u])
            hidden = (gate * sigmoid(gate) * dot(rows, exv[u])).astype(BF16)
            term = dot(hidden, cov[u])
            total = term if total is None else total + term
        part_s[at : at + size, :] = total * weight

    def gather(buf, chunk):
        def copy(k, j):
            source = (NZ - k) % NZ if k < FAR else k - FAR
            target = (source + NZ - 1) % NZ if k < FAR else source + 1
            part = pl.ds(j * chunk, chunk)
            return remote(
                buf.at[source, part], buf.at[target, part], ags, agr.at[k, j], s,
                ahead if k < FAR else behind,
            )

        return copy

    def gather_step(ring, k, chunks):
        for j in range(chunks):
            ring(k, j).wait_recv()
            if k + 1 < FAR:
                ring(k + 1, j).start()
            if k < NEAR:
                ring(FAR + k, j).wait_recv()
                if k + 1 < NEAR:
                    ring(FAR + k + 1, j).start()

    def reduce(values, chunk):
        def copy(k, j):
            part = pl.ds(j * chunk, chunk)
            return remote(
                gsend.at[k, part], grecv.at[k, part], gss, grs.at[k, j], s,
                ahead if k < FAR else behind,
            )

        def send(k, j, first):
            place = FAR - k if k < FAR else NZ - (NEAR - (k - FAR))
            rows = slice(j * chunk, (j + 1) * chunk)
            value = values(place, rows)
            if not first:
                copy(k - 1, j).wait_recv()
                value = value + grecv[k - 1, rows, :].astype(F32)
            gsend[k, rows, :] = value.astype(BF16)
            copy(k, j).start()

        return copy, send

    def reduce_rest(copy, send, chunks, start):
        for step in range(1, FAR):
            for j in range(chunks):
                if step < NEAR:
                    send(FAR + step, j, False)
                send(step, j, False)
        total = start()
        size = total.shape[0]
        for k in (FAR + NEAR - 1, FAR - 1):
            for j in range(chunks):
                copy(k, j).wait_recv()
            total = total + grecv[k, 0:size, :].astype(F32)
        return total

    sides = [(NZ - 1 - k, k + 1) if k < NEAR else (NZ - 1 - k,) for k in range(FAR)]

    @pl.when(c == 0)
    def _():
        ring = gather(x_rt, SLOTS // ACH)
        out_rt[0] = to_lines(dot(place_s[0], nz_s[0]))
        scatter_in(out_rt, x_rt)
        for copy in shared[2:]:
            copy.wait_recv()
        for j in range(ACH):
            scattered_in(out_rt, x_rt, j).wait_recv()
            ring(0, j).start()
            ring(FAR, j).start()

        def back(places):
            compute(places)
            for r in places:
                fin_rt[r] = to_lines(part_of(r))
                scatter_back(fin_rt, ret_rt, r, zis, zir.at[r])

        back((0,))
        for k in range(FAR):
            gather_step(ring, k, ACH)
            back(sides[k])
        copy, send = reduce(lambda place, rows: qz_s[place, rows, :], ROWS // ZCH)
        for r in (0, 7, 1, 6, 2, 5):
            qz_s[r] = returned(r)
        for j in range(ZCH):
            send(FAR, j, True)
        for r in (3, 4):
            qz_s[r] = returned(r)
        for j in range(ZCH):
            send(0, j, True)
        routed = reduce_rest(copy, send, ZCH, lambda: qz_s[0])
        out_ref[...] = (hmid_s[...] + rms(routed, postmix_ref[...])).astype(BF16)
        all_but_own(out_rt, x_rt, 0, zos, xir.at[0]).wait_send()
        most = pl.ds(0, SLOTS - CAP)
        remote(
            fin_rt.at[:, most], ret_rt.at[:, most], zis, zir.at[0], lax.rem(s + 1, NS), t
        ).wait_send()
        around = pl.ds(0, FAR + NEAR)
        remote(x_rt.at[around], x_rt.at[around], ags, agr.at[0, 0], s, ahead).wait_send()
        rows = pl.ds(0, ROWS)
        remote(gsend.at[:, rows], grecv.at[:, rows], gss, grs.at[0, 0], s, ahead).wait_send()

    @pl.when(c == 1)
    def _():
        ring = gather(nz_s, ROWS // ZCH)
        for j in range(ZCH):
            ring(0, j).start()
            ring(FAR, j).start()

        def dispatch(r):
            out_rt[r] = to_lines(dot(place_s[r], nz_s[r]))
            scatter(out_rt, x_rt, r, zos, zor.at[r])

        def work(places):
            for r in places:
                all_but_own(out_rt, x_rt, r, zos, zor.at[r]).wait_recv()
            compute(places)

        dispatch(0)
        for copy in shared[2:]:
            copy.wait_recv()
        for k in range(FAR):
            gather_step(ring, k, ZCH)
            for r in sides[k]:
                dispatch(r)
            if k == 1:
                work((0,))
            elif k == 2:
                work(sides[0])
        copy, send = reduce(
            lambda place, rows: part_s[
                PLACE[place] * SLOTS + rows.start : PLACE[place] * SLOTS + rows.stop, :
            ],
            SLOTS // GCH,
        )
        work(sides[1])
        work(sides[2])
        for j in range(GCH):
            send(FAR, j, True)
        work(sides[3])
        for j in range(GCH):
            send(0, j, True)
        final = reduce_rest(copy, send, GCH, lambda: part_of(0))
        fin_rt[0] = to_lines(final)
        scatter(fin_rt, ret_rt, 0, zis, zir.at[0])
        routed = returned(0)
        out_ref[...] = (hmid_s[...] + rms(routed, postmix_ref[...])).astype(BF16)
        most = pl.ds(0, SLOTS - CAP)
        remote(
            out_rt.at[:, most], x_rt.at[:, most], zos, zor.at[0], lax.rem(s + 1, NS), t
        ).wait_send()
        all_but_own(fin_rt, ret_rt, 0, zis, zir.at[0]).wait_send()
        around = pl.ds(0, FAR + NEAR)
        remote(nz_s.at[around], nz_s.at[around], ags, agr.at[0, 0], s, ahead).wait_send()
        remote(gsend, grecv, gss, grs.at[0, 0], s, ahead).wait_send()

    remote(
        buf1.at[pl.ds(0, NX - 1)], buf1.at[pl.ds(0, NX - 1)], s1s, s1r.at[0], s, sibling
    ).wait_send()
    for d in range(1, NY):
        @pl.when(y + d < NY)
        def _():
            along_y(d).wait_send()
    shared_groups().wait_send()
    for copy in shared:
        copy.wait_send()
    swap.wait_send()
    remote(dsend, drecv, dss, drs.at[0, 0], s, ahead).wait_send()


def shards(
    ask_left, keep_left, gap_left, ask_right, keep_right, gap_right, payload, switch_logits,
    keep_bias, lanewise, alpha, beta, skip, post, pre, postmix, router, switch, expansion,
    contraction, cluster,
):
    inputs = (
        keep_left, keep_right, gap_left.reshape(1, -1), gap_right.reshape(1, -1), keep_bias.T,
        cluster.reshape(1, -1), ask_left, ask_right, payload, switch_logits,
        lanewise.reshape(1, -1), skip, post.reshape(1, -1), pre.reshape(1, -1),
        postmix.reshape(1, -1), router.T,
    )
    vmem = pl.BlockSpec(memory_space=pltpu.VMEM)
    hbm = pl.BlockSpec(memory_space=pl.ANY)
    ring = FAR + NEAR
    dma = pltpu.SemaphoreType.DMA
    return pl.pallas_call(
        kernel,
        out_shape=pltpu.VMEM((ROWS, D), BF16),
        in_specs=[hbm] * 21,
        out_specs=vmem,
        scratch_shapes=[
            *(pltpu.VMEM(a.shape, a.dtype) for a in inputs),
            dma((16,)),
            pltpu.VMEM((TOK, KT), F32),
            pltpu.VMEM((TOK, KT), F32),
            pltpu.VMEM((TOK, KT), BF16),
            pltpu.VMEM((TOK, KT), BF16),
            pltpu.VMEM((TOK, KT), BF16),
            pltpu.VMEM((TOK, 128), F32),
            pltpu.VMEM((NX, 72, KT), BF16),
            pltpu.VMEM((NY, 72, KT), BF16),
            pltpu.VMEM((64, KT), F32),
            pltpu.VMEM((2, TOK // 2, 128), BF16),
            pltpu.VMEM((TOK // 2, 128), BF16),
            pltpu.VMEM((2, 128, D), BF16),
            pltpu.VMEM((TOK // 2, D), F32),
            pltpu.VMEM((ring, ROWS, D), BF16),
            pltpu.VMEM((ring, ROWS, D), BF16),
            pltpu.VMEM((ROWS, D), F32),
            pltpu.VMEM((NZ, SLOTS, LINES, 128), BF16),
            pltpu.VMEM((NZ, SLOTS, LINES, 128), BF16),
            pltpu.VMEM((SLOTS * PITCH, 128), F32),
            pltpu.VMEM((NZ * SLOTS, D), BF16),
            pltpu.VMEM((NZ * SLOTS, D), F32),
            pltpu.VMEM((2, D, HID), BF16),
            pltpu.VMEM((2, D, HID), BF16),
            pltpu.VMEM((2, HID, D), BF16),
            pltpu.VMEM((ring, SLOTS, D), BF16),
            pltpu.VMEM((ring, SLOTS, D), BF16),
            pltpu.VMEM((NZ, SLOTS, LINES, 128), BF16),
            pltpu.VMEM((NZ, SLOTS, LINES, 128), BF16),
            pltpu.VMEM((NZ, 8, 128), F32),
            pltpu.VMEM((NZ, SLOTS, ROWS), BF16),
            pltpu.VMEM((NZ, ROWS, SLOTS), BF16),
            pltpu.VMEM((NZ, ROWS, D), BF16),
            pltpu.VMEM((NZ, ROWS, D), F32),
            dma, dma,
            dma, dma((NZ,)), dma, dma((NZ,)), dma((ACH,)),
            dma((5,)), dma((5,)), dma((5,)),
            dma, dma((NX,)), dma((NY,)), dma((NY,)),
            dma, dma,
            dma, dma((ring, DCH)),
            dma, dma((ring, max(ACH, ZCH))),
            dma, dma((ring, GCH)),
        ],
        compiler_params=pltpu.CompilerParams(
            collective_id=0, has_side_effects=True, vmem_limit_bytes=56 * 1024 * 1024
        ),
    )(
        *inputs, alpha, beta, switch, expansion, contraction,
    )


def solution(mesh):
    placed = (
        P("sp", "tp"),
        P("sp", "tp"),
        P("tp"),
        P("sp", "tp"),
        P("sp", "tp"),
        P("tp"),
        P("sp", "tp"),
        P("sp", "tp"),
        P("sp", "tp"),
        P(),
        P("tp", None),
        P("tp", None),
        P(("sp", "tp"), None),
        P(),
        P(),
        P(),
        P(None, "sp"),
        P("sp", None, "tp"),
        P("sp", None, "tp"),
        P("sp", "tp", None),
        P(("sp", "tp")),
    )
    return jax.shard_map(
        shards, mesh=mesh, in_specs=placed, out_specs=P(("sp", "tp"), None), check_vma=False
    )
```

time: 89.8 us -> 80.2 us (0.89)
  Pallas kernels: 88 us -> 79.5 us
  local copies, waits for them, and re-layouts: 1.57 us -> 0.66 us
    pallas_call x1, Pallas kernels: 88 us -> 79.5 us  [shards(): pl.pallas_call(kernel, out_shape=pltpu.VMEM((ROWS, D), BF16), in_specs=[h...]
    unnamed x1, local copies, waits for them, and re-layouts: 1.57 us -> 0.66 us
where the time goes in v2:
time: 80.2 us
  Pallas kernels  79.5 us (99%)
    pallas_call x1, Pallas kernels, shards(): pl.pallas_call(kernel, out_shape=pltpu.VMEM((ROWS, D), BF16), in_specs=[h...  79.5 us

profile of v2, /device:TPU:2, one launch (start us, length us, event | category | flops | bytes accessed | tf_op | source)
XLA Modules:
  0.0 80.2 jit_solution(3704776036199762252)
XLA Ops:
  0.0 79.5 %shard_map.199 = bf16[32,2048]{1,0:T(8,128)(2,1)S(1)} custom-call(bf16[512,128]{1,0:T(8,128)(2,1)} %fa_hbm.1, bf16[512,256]{1,0:T(8,128)(2,1)} %fb_hbm.1, f32[1,128]{1,0:T(1,128)} %bitcast.15, f32[1,256]{1,0:T(1,128)} %bitcast.14, f32[2,512]{1,0:T(2,128)} %bitcast.13, s32[1,32]{1,0:T(1,128)} %bitcast.16, bf16[512,128]{1,0:T(8,128)(2,1)} %qa_hbm.1, ...), custom_call_target="tpu_custom_call" | custom-call | tf_op jit(solution)/shard_map/pallas_call | solution.py:642
  79.5 0.7 copy.23

commit v3 on v2

--- a/solution.py
+++ b/solution.py
@@ -25,7 +25,7 @@
     ((dy, dx) for dy in range(NY) for dx in range(NX)),
     key=lambda o: min(o[0], NY - o[0]) + min(o[1], NX - o[1]),
 )
-DCH, GCH, ZCH, ACH = 4, 6, 4, 4
+DCH, GCH, ZCH, ACH = 8, 6, 4, 8
 MESH = pl.DeviceIdType.MESH
 F32, BF16 = jnp.float32, jnp.bfloat16
 
@@ -136,22 +136,24 @@
     lower = jnp.where(iota((128, 128), 0) >= iota((128, 128), 1), 1.0, 0.0).astype(BF16)
 
     def decays(r, carry):
-        rows = pl.ds(pl.multiple_of(r * 128, 128), 128)
+        rows = slice(r * 128, r * 128 + 128)
         forget = jnp.concatenate([fa_ref[rows, :].astype(F32), fb_ref[rows, :].astype(F32)], axis=1)
         key = gap * sigmoid(-forget)
         left = jnp.broadcast_to(bias_ref[0:1, rows], (128, 128)).T
         right = jnp.broadcast_to(bias_ref[1:2, rows], (128, 128)).T
         logf = jnp.log1p(-key) + jnp.concatenate([left, right, right], axis=1)
-        high, mid, low = split3(logf)
-        inside = dot(lower, high) + dot(lower, mid) + dot(lower, low) + carry
+        high, mid, _ = split3(logf)
+        inside = dot(lower, high) + dot(lower, mid) + carry
         key_s[rows, :] = key
         ins_s[rows, :] = inside
         return inside[127:128, :]
 
-    last = lax.fori_loop(0, TOK // 128, decays, jnp.zeros((1, KT), F32))
+    last = jnp.zeros((1, KT), F32)
+    for r in range(TOK // 128):
+        last = decays(r, last)
 
     def scaled(r, carry):
-        rows = pl.ds(pl.multiple_of(r * 128, 128), 128)
+        rows = slice(r * 128, r * 128 + 128)
         ask = jnp.concatenate([qa_ref[rows, :].astype(F32), qb_ref[rows, :].astype(F32)], axis=1)
         key = key_s[rows, :]
         inside = ins_s[rows, :]
@@ -162,7 +164,8 @@
 
     for copy in inputs[6:9]:
         copy.wait()
-    lax.fori_loop(0, TOK // 128, scaled, 0)
+    for r in range(TOK // 128):
+        scaled(r, 0)
     summed = dot_tn(v_ref[...], wk_s[...])
     state = jnp.concatenate([summed[0:64, 0:128], summed[64:128, 128:KT]], axis=1)
 
@@ -251,7 +254,7 @@
     def from_y(k):
         return remote(buf2.at[k], buf2.at[k], s2s.at[0], s2r.at[k], k * NX + x, t)
 
-    for d in range(1, NY):
+    for d in (2, 3, 1):
         @pl.when(y + d < NY)
         def _():
             along_y(d).start()
@@ -295,24 +298,29 @@
     swap.wait_recv()
     p_s[...] = p_s[...] + dot(hrecv[...], wproj[1])
 
-    HALF = ROWS // DCH
+    PIECE = 8
+
+    def piece_d(j):
+        return j // 2 * PIECE, slice(j % 2 * (D // 2), (j % 2 + 1) * (D // 2))
 
     def ring_d(k, j):
-        part = pl.ds(j * HALF, HALF)
+        first, columns = piece_d(j)
+        part = (k, pl.ds(first, PIECE), pl.ds(columns.start, D // 2))
         return remote(
-            dsend.at[k, part], drecv.at[k, part], dss, drs.at[k, j], s,
+            dsend.at[part], drecv.at[part], dss, drs.at[k, j], s,
             ahead if k < FAR else behind,
         )
 
-    def send_d(k, j, first):
+    def send_d(k, j, starts):
         place = FAR - k if k < FAR else -(NEAR - (k - FAR))
         target = lax.rem(z + way * place + NZ, NZ)
-        rows = pl.ds(pl.multiple_of(target * ROWS + j * HALF, HALF), HALF)
-        value = p_s[rows, :]
-        if not first:
+        first, columns = piece_d(j)
+        rows = pl.ds(pl.multiple_of(target * ROWS + first, PIECE), PIECE)
+        value = p_s[rows, columns]
+        if not starts:
             ring_d(k - 1, j).wait_recv()
-            value = value + drecv[k - 1, j * HALF : (j + 1) * HALF, :].astype(F32)
-        dsend[k, j * HALF : (j + 1) * HALF, :] = value.astype(BF16)
+            value = value + drecv[k - 1, first : first + PIECE, columns].astype(F32)
+        dsend[k, first : first + PIECE, columns] = value.astype(BF16)
         ring_d(k, j).start()
 
     def slots_of(r, carry):
@@ -439,21 +447,28 @@
     def part_of(r):
         return part_s[PLACE[r] * SLOTS : PLACE[r] * SLOTS + SLOTS, :]
 
-    def compute(places):
+    def hidden_of(places):
         for place in places:
             from_lines(x_rt[place], PLACE[place] * SLOTS)
-        at, size = PLACE[places[0]] * SLOTS, SLOTS * len(places)
-        rows = x_s[at : at + size, :]
+        at = PLACE[places[0]] * SLOTS
+        rows = x_s[at : at + SLOTS * len(places), :]
         scores = sigmoid(dot_nt(rows, router))
         first, second = scores[:, 0:1], scores[:, 1:2]
         weight = jnp.where(member == 0, first, second) / (first + second)
-        total = None
+        hidden = []
         for u in range(2):
             gate = dot(rows, swv[u])
-            hidden = (gate * sigmoid(gate) * dot(rows, exv[u])).astype(BF16)
-            term = dot(hidden, cov[u])
-            total = term if total is None else total + term
-        part_s[at : at + size, :] = total * weight
+            hidden.append((gate * sigmoid(gate) * dot(rows, exv[u])).astype(BF16))
+        return places, weight, hidden
+
+    def contract(found):
+        places, weight, hidden = found
+        at = PLACE[places[0]] * SLOTS
+        total = dot(hidden[0], cov[0]) + dot(hidden[1], cov[1])
+        part_s[at : at + SLOTS * len(places), :] = total * weight
+
+    def compute(places):
+        contract(hidden_of(places))
 
     def gather(buf, chunk):
         def copy(k, j):
@@ -467,7 +482,7 @@
 
         return copy
 
-    def gather_step(ring, k, chunks):
+    def gather_step(ring, k, chunks, meanwhile=()):
         for j in range(chunks):
             ring(k, j).wait_recv()
             if k + 1 < FAR:
@@ -476,6 +491,8 @@
                 ring(FAR + k, j).wait_recv()
                 if k + 1 < NEAR:
                     ring(FAR + k + 1, j).start()
+            if j < len(meanwhile):
+                meanwhile[j]()
 
     def reduce(values, chunk):
         def copy(k, j):
@@ -526,15 +543,25 @@
             ring(FAR, j).start()
 
         def back(places):
-            compute(places)
             for r in places:
                 fin_rt[r] = to_lines(part_of(r))
                 scatter_back(fin_rt, ret_rt, r, zis, zir.at[r])
 
+        compute((0,))
         back((0,))
-        for k in range(FAR):
-            gather_step(ring, k, ACH)
-            back(sides[k])
+        gather_step(ring, 0, ACH)
+        for k in range(1, FAR):
+            found = []
+            gather_step(
+                ring, k, ACH,
+                (
+                    lambda: found.append(hidden_of(sides[k - 1])),
+                    lambda: contract(found[0]),
+                    lambda: back(sides[k - 1]),
+                ),
+            )
+        compute(sides[FAR - 1])
+        back(sides[FAR - 1])
         copy, send = reduce(lambda place, rows: qz_s[place, rows, :], ROWS // ZCH)
         for r in (0, 7, 1, 6, 2, 5):
             qz_s[r] = returned(r)
@@ -581,15 +608,13 @@
                 dispatch(r)
             if k == 1:
                 work((0,))
-            elif k == 2:
-                work(sides[0])
         copy, send = reduce(
             lambda place, rows: part_s[
                 PLACE[place] * SLOTS + rows.start : PLACE[place] * SLOTS + rows.stop, :
             ],
             SLOTS // GCH,
         )
-        work(sides[1])
+        work(sides[0] + sides[1])
         work(sides[2])
         for j in range(GCH):
             send(FAR, j, True)

time: 80.2 us -> 79.3 us (0.989); the launches traced: 80.2 us -> 77.9 us
  Pallas kernels: 79.5 us -> 77.2 us
    pallas_call x1, Pallas kernels: 79.5 us -> 77.2 us  [shards(): pl.pallas_call(kernel, out_shape=pltpu.VMEM((ROWS, D), BF16), in_specs=[h...]
where the time goes in v3:
time: 79.3 us; the launch traced here: 77.9 us
  Pallas kernels  77.2 us (97%)
    pallas_call x1, Pallas kernels, shards(): pl.pallas_call(kernel, out_shape=pltpu.VMEM((ROWS, D), BF16), in_specs=[h...  77.2 us

profile of v3, /device:TPU:2, one launch (start us, length us, event | category | flops | bytes accessed | tf_op | source)
XLA Modules:
  0.0 77.9 jit_solution(5677889000646970255)
XLA Ops:
  0.0 77.2 %shard_map.199 = bf16[32,2048]{1,0:T(8,128)(2,1)S(1)} custom-call(bf16[512,128]{1,0:T(8,128)(2,1)} %fa_hbm.1, bf16[512,256]{1,0:T(8,128)(2,1)} %fb_hbm.1, f32[1,128]{1,0:T(1,128)} %bitcast.15, f32[1,256]{1,0:T(1,128)} %bitcast.14, f32[2,512]{1,0:T(2,128)} %bitcast.13, s32[1,32]{1,0:T(1,128)} %bitcast.16, bf16[512,128]{1,0:T(8,128)(2,1)} %qa_hbm.1, ...), custom_call_target="tpu_custom_call" | custom-call | tf_op jit(solution)/shard_map/pallas_call | solution.py:667
  77.2 0.7 copy.23

commit v4 on v3

--- a/solution.py
+++ b/solution.py
@@ -25,7 +25,8 @@
     ((dy, dx) for dy in range(NY) for dx in range(NX)),
     key=lambda o: min(o[0], NY - o[0]) + min(o[1], NX - o[1]),
 )
-DCH, GCH, ZCH, ACH = 8, 6, 4, 8
+PIECE = 8
+DCH, GCH, ZCH, ACH = 8, 6, 8, 8
 MESH = pl.DeviceIdType.MESH
 F32, BF16 = jnp.float32, jnp.bfloat16
 
@@ -72,8 +73,8 @@
     key_s, ins_s, qd_s, kg_s, wk_s, intra_s, buf1, buf2, row_s, hd_s, hrecv, wproj, p_s,
     dsend, drecv, hmid_s, out_rt, x_rt, conv_s, x_s, part_s, swv, exv, cov, gsend, grecv, ret_rt, fin_rt,
     clus_s, place_s, unplace_s, nz_s, qz_s,
-    cls, clr, zos, zor, zis, zir, xir,
-    wsem, wssem, wrsem, s1s, s1r, s2s, s2r, hs, hr, dss, drs, ags, agr, gss, grs,
+    plane_sem, cls, clr, zos, zor, zis, xir,
+    wsem, wssem, wrsem, s1s, s1r, s2s, s2r, hs, hr, dss, drs, ags, agr, gss,
 ):
     s = lax.axis_index("sp")
     t = lax.axis_index("tp")
@@ -91,20 +92,11 @@
         )
 
     barrier = pltpu.get_barrier_semaphore()
-
-    def greet(d, carry):
-        pl.semaphore_signal(barrier, inc=1, device_id=(lax.rem(s + d, NS), t), device_id_type=MESH)
-        return carry
-
-    lax.fori_loop(1, NS, greet, 0)
-
-    def greet_z(d, carry):
-        peer = lax.rem(z + d, NZ) * 2 + c
-        pl.semaphore_signal(barrier, inc=1, device_id=(s, peer), device_id_type=MESH)
-        return carry
-
-    lax.fori_loop(1, NZ, greet_z, 0)
-    pl.semaphore_signal(barrier, inc=1, device_id=(s, sibling), device_id_type=MESH)
+    row = [(y * NX + lax.rem(x + d, NX), t) for d in range(1, NX)]
+    column = [(lax.rem(y + d, NY) * NX + x, t) for d in range(1, NY)]
+    near = [*row, *column, (s, ahead), (s, behind), (s, sibling)]
+    for peer in near:
+        pl.semaphore_signal(barrier, inc=1, device_id=peer, device_id_type=MESH)
 
     inputs = [
         pltpu.make_async_copy(a, b, insem.at[k])
@@ -152,20 +144,20 @@
     for r in range(TOK // 128):
         last = decays(r, last)
 
-    def scaled(r, carry):
+    def weighted(r):
+        rows = slice(r * 128, r * 128 + 128)
+        wk_s[rows, :] = (key_s[rows, :] * jnp.exp(last - ins_s[rows, :])).astype(BF16)
+
+    def scaled(r):
         rows = slice(r * 128, r * 128 + 128)
         ask = jnp.concatenate([qa_ref[rows, :].astype(F32), qb_ref[rows, :].astype(F32)], axis=1)
-        key = key_s[rows, :]
         inside = ins_s[rows, :]
         qd_s[rows, :] = (ask * sigmoid(ask) * jnp.exp(inside)).astype(BF16)
-        kg_s[rows, :] = (key * jnp.exp(-inside)).astype(BF16)
-        wk_s[rows, :] = (key * jnp.exp(last - inside)).astype(BF16)
-        return carry
-
-    for copy in inputs[6:9]:
-        copy.wait()
+        kg_s[rows, :] = (key_s[rows, :] * jnp.exp(-inside)).astype(BF16)
+
     for r in range(TOK // 128):
-        scaled(r, 0)
+        weighted(r)
+    inputs[8].wait()
     summed = dot_tn(v_ref[...], wk_s[...])
     state = jnp.concatenate([summed[0:64, 0:128], summed[64:128, 128:KT]], axis=1)
 
@@ -181,9 +173,11 @@
         return buf[place, 0:64, :].astype(F32), lines[0:1] + lines[1:2] + lines[2:3]
 
     packed(buf1, x, state, last)
-    clus_s[z] = jnp.zeros((8, 128), F32)
-    clus_s[z, :, 0:ROWS] = jnp.broadcast_to(cluster_ref[...].astype(F32), (8, ROWS))
-    pl.semaphore_wait(barrier, NS - 1 + NZ)
+    clus_s[0] = jnp.zeros((8, 128), F32)
+    clus_s[0, :, 0:ROWS] = jnp.broadcast_to(cluster_ref[...].astype(F32), (8, ROWS))
+    pl.semaphore_wait(barrier, len(near))
+    for peer in row:
+        pl.semaphore_signal(plane_sem, inc=1, device_id=peer, device_id_type=MESH)
 
     def along_x(d):
         return remote(buf1.at[x], buf1.at[x], s1s, s1r.at[x], y * NX + lax.rem(x + d, NX), t)
@@ -203,23 +197,6 @@
     for copy in shared[:4]:
         copy.start()
 
-    def share_groups(d):
-        return remote(
-            clus_s.at[z], clus_s.at[z], cls, clr, s, lax.rem(z + d, NZ) * 2 + c
-        )
-
-    def shared_groups():
-        most = pl.ds(0, NZ - 1)
-        return remote(clus_s.at[most], clus_s.at[most], cls, clr, s, ahead)
-
-    def each(action, count=NS):
-        def body(d, carry):
-            action(d)
-            return carry
-
-        lax.fori_loop(1, count, body, 0)
-
-    each(lambda d: share_groups(d).start(), NZ)
     left_half = iota((256, 128), 1) < 64
 
     def intra(columns, first):
@@ -231,8 +208,10 @@
             found = dot(scores, v_ref[0:width, :])
             intra_s[rows, :] = found if first else jnp.where(left_half, intra_s[rows, :], found)
 
-    for copy in inputs[9:]:
+    for copy in inputs[6:8] + inputs[9:]:
         copy.wait()
+    for r in range(TOK // 128):
+        scaled(r)
     intra(slice(0, 128), True)
 
     for d in range(1, NX):
@@ -298,8 +277,6 @@
     swap.wait_recv()
     p_s[...] = p_s[...] + dot(hrecv[...], wproj[1])
 
-    PIECE = 8
-
     def piece_d(j):
         return j // 2 * PIECE, slice(j % 2 * (D // 2), (j % 2 + 1) * (D // 2))
 
@@ -323,9 +300,31 @@
         dsend[k, first : first + PIECE, columns] = value.astype(BF16)
         ring_d(k, j).start()
 
-    def slots_of(r, carry):
-        there = lax.rem(z + way * r + NZ, NZ)
-        group_row = jnp.broadcast_to(clus_s[there, 0:1, 0:ROWS], (ROWS, ROWS))
+    def gather(buf, part, ssem, rsem):
+        def copy(k, j):
+            source = (NZ - k) % NZ if k < FAR else k - FAR
+            target = (source + NZ - 1) % NZ if k < FAR else source + 1
+            return remote(
+                buf.at[(source, *part(j))], buf.at[(target, *part(j))], ssem, rsem.at[k, j], s,
+                ahead if k < FAR else behind,
+            )
+
+        return copy
+
+    def gather_step(ring, k, chunks, meanwhile=()):
+        for j in range(chunks):
+            ring(k, j).wait_recv()
+            if k + 1 < FAR:
+                ring(k + 1, j).start()
+            if k < NEAR:
+                ring(FAR + k, j).wait_recv()
+                if k + 1 < NEAR:
+                    ring(FAR + k + 1, j).start()
+            if j < len(meanwhile):
+                meanwhile[j]()
+
+    def slots_of(r):
+        group_row = jnp.broadcast_to(clus_s[r, 0:1, 0:ROWS], (ROWS, ROWS))
         diagonal = iota((ROWS, ROWS), 0) == iota((ROWS, ROWS), 1)
         group_column = jnp.sum(jnp.where(diagonal, group_row, 0.0), axis=1, keepdims=True)
         same = jnp.where(group_row == group_column, 1.0, 0.0)
@@ -341,17 +340,25 @@
         unplace_s[r] = jnp.where(
             iota((ROWS, SLOTS), 1).astype(F32) == slot_column, 1.0, 0.0
         ).astype(BF16)
-        return carry
-
+
+    groups = gather(clus_s, lambda j: (), cls, clr)
+    groups(0, 0).start()
+    groups(FAR, 0).start()
     for step in range(FAR):
+        if step:
+            gather_step(groups, step - 1, 1)
         for j in range(DCH):
             send_d(step, j, step == 0)
             if step < NEAR:
                 send_d(FAR + step, j, step == 0)
         if step == 0:
             shared[4].start()
-            shared_groups().wait_recv()
-            lax.fori_loop(0, NZ, slots_of, 0)
+            slots_of(0)
+        else:
+            slots_of(NZ - step)
+            slots_of(step)
+    gather_step(groups, FAR - 1, 1)
+    slots_of(FAR)
     mixed = p_s[pl.ds(pl.multiple_of(z * ROWS, ROWS), ROWS), :]
     for k in (FAR + NEAR - 1, FAR - 1):
         for j in range(DCH):
@@ -429,8 +436,8 @@
             remote(src.at[r, near_slots(p)], dst.at[r, own], ssem, rsem, there, t).start()
         dst[r, own] = src[r, 0:CAP]
 
-    def returned(r):
-        all_but_own(fin_rt, ret_rt, r, zis, zir.at[r]).wait_recv()
+    def returned(r, rsem):
+        all_but_own(fin_rt, ret_rt, r, zis, rsem).wait_recv()
         at = PLACE[r] * SLOTS
         from_lines(ret_rt[r], at)
         return dot(unplace_s[r], x_s[at : at + SLOTS, :])
@@ -470,46 +477,28 @@
     def compute(places):
         contract(hidden_of(places))
 
-    def gather(buf, chunk):
+    def part_z(j):
+        first, columns = piece_d(j)
+        return pl.ds(first, PIECE), pl.ds(columns.start, D // 2)
+
+    def part_g(j):
+        return pl.ds(j * PIECE, PIECE), pl.ds(0, D)
+
+    def reduce(values, part):
         def copy(k, j):
-            source = (NZ - k) % NZ if k < FAR else k - FAR
-            target = (source + NZ - 1) % NZ if k < FAR else source + 1
-            part = pl.ds(j * chunk, chunk)
             return remote(
-                buf.at[source, part], buf.at[target, part], ags, agr.at[k, j], s,
+                gsend.at[(k, *part(j))], grecv.at[(k, *part(j))], gss, drs.at[k, j], s,
                 ahead if k < FAR else behind,
             )
 
-        return copy
-
-    def gather_step(ring, k, chunks, meanwhile=()):
-        for j in range(chunks):
-            ring(k, j).wait_recv()
-            if k + 1 < FAR:
-                ring(k + 1, j).start()
-            if k < NEAR:
-                ring(FAR + k, j).wait_recv()
-                if k + 1 < NEAR:
-                    ring(FAR + k + 1, j).start()
-            if j < len(meanwhile):
-                meanwhile[j]()
-
-    def reduce(values, chunk):
-        def copy(k, j):
-            part = pl.ds(j * chunk, chunk)
-            return remote(
-                gsend.at[k, part], grecv.at[k, part], gss, grs.at[k, j], s,
-                ahead if k < FAR else behind,
-            )
-
         def send(k, j, first):
             place = FAR - k if k < FAR else NZ - (NEAR - (k - FAR))
-            rows = slice(j * chunk, (j + 1) * chunk)
-            value = values(place, rows)
+            rows, columns = (slice(d.start, d.start + d.size) for d in part(j))
+            value = values(place, rows, columns)
             if not first:
                 copy(k - 1, j).wait_recv()
-                value = value + grecv[k - 1, rows, :].astype(F32)
-            gsend[k, rows, :] = value.astype(BF16)
+                value = value + grecv[k - 1, rows, columns].astype(F32)
+            gsend[k, rows, columns] = value.astype(BF16)
             copy(k, j).start()
 
         return copy, send
@@ -530,9 +519,11 @@
 
     sides = [(NZ - 1 - k, k + 1) if k < NEAR else (NZ - 1 - k,) for k in range(FAR)]
 
+    pl.semaphore_wait(plane_sem, NX - 1)
+
     @pl.when(c == 0)
     def _():
-        ring = gather(x_rt, SLOTS // ACH)
+        ring = gather(x_rt, lambda j: (pl.ds(j * (SLOTS // ACH), SLOTS // ACH),), ags, agr)
         out_rt[0] = to_lines(dot(place_s[0], nz_s[0]))
         scatter_in(out_rt, x_rt)
         for copy in shared[2:]:
@@ -545,7 +536,7 @@
         def back(places):
             for r in places:
                 fin_rt[r] = to_lines(part_of(r))
-                scatter_back(fin_rt, ret_rt, r, zis, zir.at[r])
+                scatter_back(fin_rt, ret_rt, r, zis, zor.at[r])
 
         compute((0,))
         back((0,))
@@ -562,13 +553,13 @@
             )
         compute(sides[FAR - 1])
         back(sides[FAR - 1])
-        copy, send = reduce(lambda place, rows: qz_s[place, rows, :], ROWS // ZCH)
+        copy, send = reduce(lambda place, rows, columns: qz_s[place, rows, columns], part_z)
         for r in (0, 7, 1, 6, 2, 5):
-            qz_s[r] = returned(r)
+            qz_s[r] = returned(r, zor.at[r])
         for j in range(ZCH):
             send(FAR, j, True)
         for r in (3, 4):
-            qz_s[r] = returned(r)
+            qz_s[r] = returned(r, zor.at[r])
         for j in range(ZCH):
             send(0, j, True)
         routed = reduce_rest(copy, send, ZCH, lambda: qz_s[0])
@@ -576,16 +567,16 @@
         all_but_own(out_rt, x_rt, 0, zos, xir.at[0]).wait_send()
         most = pl.ds(0, SLOTS - CAP)
         remote(
-            fin_rt.at[:, most], ret_rt.at[:, most], zis, zir.at[0], lax.rem(s + 1, NS), t
+            fin_rt.at[:, most], ret_rt.at[:, most], zis, zor.at[0], lax.rem(s + 1, NS), t
         ).wait_send()
         around = pl.ds(0, FAR + NEAR)
         remote(x_rt.at[around], x_rt.at[around], ags, agr.at[0, 0], s, ahead).wait_send()
         rows = pl.ds(0, ROWS)
-        remote(gsend.at[:, rows], grecv.at[:, rows], gss, grs.at[0, 0], s, ahead).wait_send()
+        remote(gsend.at[:, rows], grecv.at[:, rows], gss, drs.at[0, 0], s, ahead).wait_send()
 
     @pl.when(c == 1)
     def _():
-        ring = gather(nz_s, ROWS // ZCH)
+        ring = gather(nz_s, part_z, ags, agr)
         for j in range(ZCH):
             ring(0, j).start()
             ring(FAR, j).start()
@@ -609,10 +600,10 @@
             if k == 1:
                 work((0,))
         copy, send = reduce(
-            lambda place, rows: part_s[
-                PLACE[place] * SLOTS + rows.start : PLACE[place] * SLOTS + rows.stop, :
+            lambda place, rows, columns: part_s[
+                PLACE[place] * SLOTS + rows.start : PLACE[place] * SLOTS + rows.stop, columns
             ],
-            SLOTS // GCH,
+            part_g,
         )
         work(sides[0] + sides[1])
         work(sides[2])
@@ -623,17 +614,17 @@
             send(0, j, True)
         final = reduce_rest(copy, send, GCH, lambda: part_of(0))
         fin_rt[0] = to_lines(final)
-        scatter(fin_rt, ret_rt, 0, zis, zir.at[0])
-        routed = returned(0)
+        scatter(fin_rt, ret_rt, 0, zis, xir.at[0])
+        routed = returned(0, xir.at[0])
         out_ref[...] = (hmid_s[...] + rms(routed, postmix_ref[...])).astype(BF16)
         most = pl.ds(0, SLOTS - CAP)
         remote(
             out_rt.at[:, most], x_rt.at[:, most], zos, zor.at[0], lax.rem(s + 1, NS), t
         ).wait_send()
-        all_but_own(fin_rt, ret_rt, 0, zis, zir.at[0]).wait_send()
+        all_but_own(fin_rt, ret_rt, 0, zis, xir.at[0]).wait_send()
         around = pl.ds(0, FAR + NEAR)
         remote(nz_s.at[around], nz_s.at[around], ags, agr.at[0, 0], s, ahead).wait_send()
-        remote(gsend, grecv, gss, grs.at[0, 0], s, ahead).wait_send()
+        remote(gsend, grecv, gss, drs.at[0, 0], s, ahead).wait_send()
 
     remote(
         buf1.at[pl.ds(0, NX - 1)], buf1.at[pl.ds(0, NX - 1)], s1s, s1r.at[0], s, sibling
@@ -642,7 +633,8 @@
         @pl.when(y + d < NY)
         def _():
             along_y(d).wait_send()
-    shared_groups().wait_send()
+    around = pl.ds(0, FAR + NEAR)
+    remote(clus_s.at[around], clus_s.at[around], cls, clr.at[0, 0], s, ahead).wait_send()
     for copy in shared:
         copy.wait_send()
     swap.wait_send()
@@ -705,14 +697,14 @@
             pltpu.VMEM((NZ, ROWS, SLOTS), BF16),
             pltpu.VMEM((NZ, ROWS, D), BF16),
             pltpu.VMEM((NZ, ROWS, D), F32),
-            dma, dma,
-            dma, dma((NZ,)), dma, dma((NZ,)), dma((ACH,)),
+            pltpu.SemaphoreType.REGULAR, dma, dma((ring, 1)),
+            dma, dma((NZ,)), dma, dma((ACH,)),
             dma((5,)), dma((5,)), dma((5,)),
             dma, dma((NX,)), dma((NY,)), dma((NY,)),
             dma, dma,
             dma, dma((ring, DCH)),
             dma, dma((ring, max(ACH, ZCH))),
-            dma, dma((ring, GCH)),
+            dma,
         ],
         compiler_params=pltpu.CompilerParams(
             collective_id=0, has_side_effects=True, vmem_limit_bytes=56 * 1024 * 1024

time: 79.3 us -> 76.9 us (0.970); the launches traced: 77.9 us -> 76.5 us
  Pallas kernels: 77.2 us -> 75.8 us
    pallas_call x1, Pallas kernels: 77.2 us -> 75.8 us  [shards(): pl.pallas_call(kernel, out_shape=pltpu.VMEM((ROWS, D), BF16), in_specs=[h...]
where the time goes in v4:
time: 76.9 us; the launch traced here: 76.5 us
  Pallas kernels  75.8 us (99%)
    pallas_call x1, Pallas kernels, shards(): pl.pallas_call(kernel, out_shape=pltpu.VMEM((ROWS, D), BF16), in_specs=[h...  75.8 us

profile of v4, /device:TPU:2, one launch (start us, length us, event | category | flops | bytes accessed | tf_op | source)
XLA Modules:
  0.0 76.5 jit_solution(12984474088961771585)
XLA Ops:
  0.0 75.8 %shard_map.199 = bf16[32,2048]{1,0:T(8,128)(2,1)S(1)} custom-call(bf16[512,128]{1,0:T(8,128)(2,1)} %fa_hbm.1, bf16[512,256]{1,0:T(8,128)(2,1)} %fb_hbm.1, f32[1,128]{1,0:T(1,128)} %bitcast.15, f32[1,256]{1,0:T(1,128)} %bitcast.14, f32[2,512]{1,0:T(2,128)} %bitcast.13, s32[1,32]{1,0:T(1,128)} %bitcast.16, bf16[512,128]{1,0:T(8,128)(2,1)} %qa_hbm.1, ...), custom_call_target="tpu_custom_call" | custom-call | tf_op jit(solution)/shard_map/pallas_call | solution.py:659
  75.8 0.7 copy.23

commit v5 on v4

--- a/solution.py
+++ b/solution.py
@@ -73,6 +73,7 @@
     key_s, ins_s, qd_s, kg_s, wk_s, intra_s, buf1, buf2, row_s, hd_s, hrecv, wproj, p_s,
     dsend, drecv, hmid_s, out_rt, x_rt, conv_s, x_s, part_s, swv, exv, cov, gsend, grecv, ret_rt, fin_rt,
     clus_s, place_s, unplace_s, nz_s, qz_s,
+    rets_rt, sends_s, recvs_s, unp_s, routs_s, routr_s, oss, rrs, us, ur, qs, qr, pair_sem,
     plane_sem, cls, clr, zos, zor, zis, xir,
     wsem, wssem, wrsem, s1s, s1r, s2s, s2r, hs, hr, dss, drs, ags, agr, gss,
 ):
@@ -353,6 +354,8 @@
                 send_d(FAR + step, j, step == 0)
         if step == 0:
             shared[4].start()
+            pl.semaphore_wait(plane_sem, NX - 1)
+            pl.semaphore_signal(pair_sem, inc=1, device_id=(s, sibling), device_id_type=MESH)
             slots_of(0)
         else:
             slots_of(NZ - step)
@@ -390,26 +393,14 @@
     def at_offset(dy, dx):
         return lax.rem(y + dy, NY) * NX + lax.rem(x + dx, NX)
 
-    def far_first(action):
-        middle = 2 * NX + 2
-
-        def body(i, carry):
-            i = i + jnp.where(i >= middle, 1, 0)
-            action(at_offset(lax.rem(2 + i // NX, NY), lax.rem(2 + lax.rem(i, NX), NX)))
-            return carry
-
-        lax.fori_loop(0, NS - 1, body, 0)
-
     def all_but_own(src, dst, r, ssem, rsem):
         most = pl.ds(0, SLOTS - CAP)
         return remote(src.at[r, most], dst.at[r, most], ssem, rsem, lax.rem(s + 1, NS), t)
 
     def scatter(src, dst, r, ssem, rsem):
-        far_first(
-            lambda there: remote(
-                src.at[r, slots_for(there)], dst.at[r, own], ssem, rsem, there, t
-            ).start()
-        )
+        for dy, dx in reversed(OFFSETS[1:]):
+            there = at_offset(dy, dx)
+            remote(src.at[r, slots_for(there)], dst.at[r, own], ssem, rsem, there, t).start()
         dst[r, own] = src[r, own]
 
     def near_slots(p):
@@ -431,10 +422,15 @@
         return remote(src.at[0, part], dst.at[0, part], zos, xir.at[q], lax.rem(s + 1, NS), t)
 
     def scatter_back(src, dst, r, ssem, rsem):
-        for p in range(NS - 1, 0, -1):
+        for p in range(NS - 1, -1, -1):
             there = at_offset(*OFFSETS[p])
-            remote(src.at[r, near_slots(p)], dst.at[r, own], ssem, rsem, there, t).start()
-        dst[r, own] = src[r, 0:CAP]
+            remote(src.at[r, near_slots(p)], dst.at[r, own], ssem, rsem, there, sibling).start()
+
+    def given_back(r):
+        remote(fin_rt.at[r], rets_rt.at[r], zis, rrs.at[r], s, sibling).wait_recv()
+        at = PLACE[r] * SLOTS
+        from_lines(rets_rt[r], at)
+        qz_s[r] = dot(unp_s[r], x_s[at : at + SLOTS, :])
 
     def returned(r, rsem):
         all_but_own(fin_rt, ret_rt, r, zis, rsem).wait_recv()
@@ -484,11 +480,11 @@
     def part_g(j):
         return pl.ds(j * PIECE, PIECE), pl.ds(0, D)
 
-    def reduce(values, part):
+    def reduce(values, part, sent, received, ssem, rsem, to=(ahead, behind)):
         def copy(k, j):
             return remote(
-                gsend.at[(k, *part(j))], grecv.at[(k, *part(j))], gss, drs.at[k, j], s,
-                ahead if k < FAR else behind,
+                sent.at[(k, *part(j))], received.at[(k, *part(j))], ssem, rsem.at[k, j], s,
+                to[0] if k < FAR else to[1],
             )
 
         def send(k, j, first):
@@ -497,32 +493,33 @@
             value = values(place, rows, columns)
             if not first:
                 copy(k - 1, j).wait_recv()
-                value = value + grecv[k - 1, rows, columns].astype(F32)
-            gsend[k, rows, columns] = value.astype(BF16)
+                value = value + received[k - 1, rows, columns].astype(F32)
+            sent[k, rows, columns] = value.astype(BF16)
             copy(k, j).start()
 
         return copy, send
 
-    def reduce_rest(copy, send, chunks, start):
-        for step in range(1, FAR):
-            for j in range(chunks):
-                if step < NEAR:
-                    send(FAR + step, j, False)
-                send(step, j, False)
-        total = start()
-        size = total.shape[0]
+    def reduce_step(send, chunks, step):
+        for j in range(chunks):
+            send(step, j, False)
+            if step < NEAR:
+                send(FAR + step, j, False)
+
+    def reduce_end(copy, received, chunks, total):
         for k in (FAR + NEAR - 1, FAR - 1):
             for j in range(chunks):
                 copy(k, j).wait_recv()
-            total = total + grecv[k, 0:size, :].astype(F32)
+            total = total + received[k].astype(F32)
         return total
 
     sides = [(NZ - 1 - k, k + 1) if k < NEAR else (NZ - 1 - k,) for k in range(FAR)]
 
-    pl.semaphore_wait(plane_sem, NX - 1)
+    pl.semaphore_wait(pair_sem, 1)
 
     @pl.when(c == 0)
     def _():
+        slots_copy = remote(unplace_s, unp_s, us, ur, s, sibling)
+        slots_copy.start()
         ring = gather(x_rt, lambda j: (pl.ds(j * (SLOTS // ACH), SLOTS // ACH),), ags, agr)
         out_rt[0] = to_lines(dot(place_s[0], nz_s[0]))
         scatter_in(out_rt, x_rt)
@@ -536,7 +533,7 @@
         def back(places):
             for r in places:
                 fin_rt[r] = to_lines(part_of(r))
-                scatter_back(fin_rt, ret_rt, r, zis, zor.at[r])
+                scatter_back(fin_rt, rets_rt, r, zis, rrs.at[r])
 
         compute((0,))
         back((0,))
@@ -553,26 +550,14 @@
             )
         compute(sides[FAR - 1])
         back(sides[FAR - 1])
-        copy, send = reduce(lambda place, rows, columns: qz_s[place, rows, columns], part_z)
-        for r in (0, 7, 1, 6, 2, 5):
-            qz_s[r] = returned(r, zor.at[r])
-        for j in range(ZCH):
-            send(FAR, j, True)
-        for r in (3, 4):
-            qz_s[r] = returned(r, zor.at[r])
-        for j in range(ZCH):
-            send(0, j, True)
-        routed = reduce_rest(copy, send, ZCH, lambda: qz_s[0])
+        remote(routs_s, routr_s, qs, qr, s, sibling).wait_recv()
+        routed = routr_s[...].astype(F32)
         out_ref[...] = (hmid_s[...] + rms(routed, postmix_ref[...])).astype(BF16)
         all_but_own(out_rt, x_rt, 0, zos, xir.at[0]).wait_send()
-        most = pl.ds(0, SLOTS - CAP)
-        remote(
-            fin_rt.at[:, most], ret_rt.at[:, most], zis, zor.at[0], lax.rem(s + 1, NS), t
-        ).wait_send()
+        slots_copy.wait_send()
+        remote(fin_rt, rets_rt, zis, rrs.at[0], s, sibling).wait_send()
         around = pl.ds(0, FAR + NEAR)
         remote(x_rt.at[around], x_rt.at[around], ags, agr.at[0, 0], s, ahead).wait_send()
-        rows = pl.ds(0, ROWS)
-        remote(gsend.at[:, rows], grecv.at[:, rows], gss, drs.at[0, 0], s, ahead).wait_send()
 
     @pl.when(c == 1)
     def _():
@@ -599,24 +584,51 @@
                 dispatch(r)
             if k == 1:
                 work((0,))
+            elif k == 2:
+                work(sides[0])
         copy, send = reduce(
             lambda place, rows, columns: part_s[
                 PLACE[place] * SLOTS + rows.start : PLACE[place] * SLOTS + rows.stop, columns
             ],
-            part_g,
+            part_g, gsend, grecv, gss, drs,
         )
-        work(sides[0] + sides[1])
+        work(sides[1])
         work(sides[2])
         for j in range(GCH):
             send(FAR, j, True)
         work(sides[3])
         for j in range(GCH):
             send(0, j, True)
-        final = reduce_rest(copy, send, GCH, lambda: part_of(0))
+        copy_s, send_s = reduce(
+            lambda place, rows, columns: qz_s[place, rows, columns], part_z, sends_s, recvs_s,
+            oss, agr, (behind, ahead),
+        )
+        remote(unplace_s, unp_s, us, ur, s, sibling).wait_recv()
+        for r in (0, 7, 1):
+            given_back(r)
+        reduce_step(send, GCH, 1)
+        for r in (6, 2):
+            given_back(r)
+        reduce_step(send, GCH, 2)
+        given_back(5)
+        for j in range(ZCH):
+            send_s(FAR, j, True)
+        given_back(3)
+        reduce_step(send, GCH, 3)
+        given_back(4)
+        for j in range(ZCH):
+            send_s(0, j, True)
+        reduce_step(send_s, ZCH, 1)
+        final = reduce_end(copy, grecv, GCH, part_of(0))
         fin_rt[0] = to_lines(final)
         scatter(fin_rt, ret_rt, 0, zis, xir.at[0])
+        reduce_step(send_s, ZCH, 2)
+        reduce_step(send_s, ZCH, 3)
         routed = returned(0, xir.at[0])
         out_ref[...] = (hmid_s[...] + rms(routed, postmix_ref[...])).astype(BF16)
+        routs_s[...] = reduce_end(copy_s, recvs_s, ZCH, qz_s[0]).astype(BF16)
+        sums_copy = remote(routs_s, routr_s, qs, qr, s, sibling)
+        sums_copy.start()
         most = pl.ds(0, SLOTS - CAP)
         remote(
             out_rt.at[:, most], x_rt.at[:, most], zos, zor.at[0], lax.rem(s + 1, NS), t
@@ -625,6 +637,8 @@
         around = pl.ds(0, FAR + NEAR)
         remote(nz_s.at[around], nz_s.at[around], ags, agr.at[0, 0], s, ahead).wait_send()
         remote(gsend, grecv, gss, drs.at[0, 0], s, ahead).wait_send()
+        remote(sends_s, recvs_s, oss, agr.at[0, 0], s, ahead).wait_send()
+        sums_copy.wait_send()
 
     remote(
         buf1.at[pl.ds(0, NX - 1)], buf1.at[pl.ds(0, NX - 1)], s1s, s1r.at[0], s, sibling
@@ -697,6 +711,13 @@
             pltpu.VMEM((NZ, ROWS, SLOTS), BF16),
             pltpu.VMEM((NZ, ROWS, D), BF16),
             pltpu.VMEM((NZ, ROWS, D), F32),
+            pltpu.VMEM((NZ, SLOTS, LINES, 128), BF16),
+            pltpu.VMEM((ring, ROWS, D), BF16),
+            pltpu.VMEM((ring, ROWS, D), BF16),
+            pltpu.VMEM((NZ, ROWS, SLOTS), BF16),
+            pltpu.VMEM((ROWS, D), BF16),
+            pltpu.VMEM((ROWS, D), BF16),
+            dma, dma((NZ,)), dma, dma, dma, dma, pltpu.SemaphoreType.REGULAR,
             pltpu.SemaphoreType.REGULAR, dma, dma((ring, 1)),
             dma, dma((NZ,)), dma, dma((ACH,)),
             dma((5,)), dma((5,)), dma((5,)),

time: 76.9 us -> 75.6 us (0.983)
  Pallas kernels: 75.8 us -> 74 us
    pallas_call x1, Pallas kernels: 75.8 us -> 74 us  [shards(): pl.pallas_call(kernel, out_shape=pltpu.VMEM((ROWS, D), BF16), in_specs=[h...]
where the time goes in v5:
time: 75.6 us; the launch traced here: 74.7 us
  Pallas kernels  74 us (98%)
    pallas_call x1, Pallas kernels, shards(): pl.pallas_call(kernel, out_shape=pltpu.VMEM((ROWS, D), BF16), in_specs=[h...  74 us

profile of v5, /device:TPU:2, one launch (start us, length us, event | category | flops | bytes accessed | tf_op | source)
XLA Modules:
  0.0 74.7 jit_solution(6640041465018969585)
XLA Ops:
  0.0 74.0 %shard_map.199 = bf16[32,2048]{1,0:T(8,128)(2,1)S(1)} custom-call(bf16[512,128]{1,0:T(8,128)(2,1)} %fa_hbm.1, bf16[512,256]{1,0:T(8,128)(2,1)} %fb_hbm.1, f32[1,128]{1,0:T(1,128)} %bitcast.15, f32[1,256]{1,0:T(1,128)} %bitcast.14, f32[2,512]{1,0:T(2,128)} %bitcast.13, s32[1,32]{1,0:T(1,128)} %bitcast.16, bf16[512,128]{1,0:T(8,128)(2,1)} %qa_hbm.1, ...), custom_call_target="tpu_custom_call" | custom-call | tf_op jit(solution)/shard_map/pallas_call | solution.py:673
  74.0 0.7 copy.23

commit v6 on v5

--- a/solution.py
+++ b/solution.py
@@ -512,6 +512,10 @@
             total = total + received[k].astype(F32)
         return total
 
+    def summed_rows(h):
+        rows = pl.ds(h * (ROWS // 2), ROWS // 2)
+        return remote(routs_s.at[rows], routr_s.at[rows], qs, qr.at[h], s, sibling)
+
     sides = [(NZ - 1 - k, k + 1) if k < NEAR else (NZ - 1 - k,) for k in range(FAR)]
 
     pl.semaphore_wait(pair_sem, 1)
@@ -550,7 +554,8 @@
             )
         compute(sides[FAR - 1])
         back(sides[FAR - 1])
-        remote(routs_s, routr_s, qs, qr, s, sibling).wait_recv()
+        for h in range(2):
+            summed_rows(h).wait_recv()
         routed = routr_s[...].astype(F32)
         out_ref[...] = (hmid_s[...] + rms(routed, postmix_ref[...])).astype(BF16)
         all_but_own(out_rt, x_rt, 0, zos, xir.at[0]).wait_send()
@@ -626,9 +631,14 @@
         reduce_step(send_s, ZCH, 3)
         routed = returned(0, xir.at[0])
         out_ref[...] = (hmid_s[...] + rms(routed, postmix_ref[...])).astype(BF16)
-        routs_s[...] = reduce_end(copy_s, recvs_s, ZCH, qz_s[0]).astype(BF16)
-        sums_copy = remote(routs_s, routr_s, qs, qr, s, sibling)
-        sums_copy.start()
+        for h in range(2):
+            rows = slice(h * (ROWS // 2), (h + 1) * (ROWS // 2))
+            for k in (FAR + NEAR - 1, FAR - 1):
+                for j in range(h * (ZCH // 2), (h + 1) * (ZCH // 2)):
+                    copy_s(k, j).wait_recv()
+            total = qz_s[0, rows, :] + recvs_s[FAR + NEAR - 1, rows, :].astype(F32)
+            routs_s[rows, :] = (total + recvs_s[FAR - 1, rows, :].astype(F32)).astype(BF16)
+            summed_rows(h).start()
         most = pl.ds(0, SLOTS - CAP)
         remote(
             out_rt.at[:, most], x_rt.at[:, most], zos, zor.at[0], lax.rem(s + 1, NS), t
@@ -638,7 +648,7 @@
         remote(nz_s.at[around], nz_s.at[around], ags, agr.at[0, 0], s, ahead).wait_send()
         remote(gsend, grecv, gss, drs.at[0, 0], s, ahead).wait_send()
         remote(sends_s, recvs_s, oss, agr.at[0, 0], s, ahead).wait_send()
-        sums_copy.wait_send()
+        remote(routs_s, routr_s, qs, qr.at[0], s, sibling).wait_send()
 
     remote(
         buf1.at[pl.ds(0, NX - 1)], buf1.at[pl.ds(0, NX - 1)], s1s, s1r.at[0], s, sibling
@@ -717,7 +727,7 @@
             pltpu.VMEM((NZ, ROWS, SLOTS), BF16),
             pltpu.VMEM((ROWS, D), BF16),
             pltpu.VMEM((ROWS, D), BF16),
-            dma, dma((NZ,)), dma, dma, dma, dma, pltpu.SemaphoreType.REGULAR,
+            dma, dma((NZ,)), dma, dma, dma, dma((2,)), pltpu.SemaphoreType.REGULAR,
             pltpu.SemaphoreType.REGULAR, dma, dma((ring, 1)),
             dma, dma((NZ,)), dma, dma((ACH,)),
             dma((5,)), dma((5,)), dma((5,)),

time: 75.6 us -> 75.5 us (level)
  no operation moved by 1% of the time
where the time goes in v6:
time: 75.5 us; the launch traced here: 74.6 us
  Pallas kernels  73.9 us (98%)
    pallas_call x1, Pallas kernels, shards(): pl.pallas_call(kernel, out_shape=pltpu.VMEM((ROWS, D), BF16), in_specs=[h...  73.9 us

profile of v6, /device:TPU:2, one launch (start us, length us, event | category | flops | bytes accessed | tf_op | source)
XLA Modules:
  0.0 74.6 jit_solution(12172831602257005681)
XLA Ops:
  0.0 73.9 %shard_map.199 = bf16[32,2048]{1,0:T(8,128)(2,1)S(1)} custom-call(bf16[512,128]{1,0:T(8,128)(2,1)} %fa_hbm.1, bf16[512,256]{1,0:T(8,128)(2,1)} %fb_hbm.1, f32[1,128]{1,0:T(1,128)} %bitcast.15, f32[1,256]{1,0:T(1,128)} %bitcast.14, f32[2,512]{1,0:T(2,128)} %bitcast.13, s32[1,32]{1,0:T(1,128)} %bitcast.16, bf16[512,128]{1,0:T(8,128)(2,1)} %qa_hbm.1, ...), custom_call_target="tpu_custom_call" | custom-call | tf_op jit(solution)/shard_map/pallas_call | solution.py:683
  73.9 0.7 copy.23
